TPU v7x, 128 devices: a whole 4x4x4 slice. The times are simulated.
128 devices in a mesh: ep: 32 (over z, y, core), tp: 4 (over x).
Axes of the slice: x: 4, y: 4, z: 4, core: 2. Of those that a mesh axis runs over, the one named last changes fastest.
Arguments:
- hidden: bfloat16 [1024, 2048], P('ep')
- norm_gains: float32 [4, 2048], replicated, may hold values from 0.1 to 1.9
- w_query: bfloat16 [2048, 1024], P(None, 'tp'), may hold values from -0.125 to 0.125
- w_key: bfloat16 [2048, 1024], P(None, 'tp'), may hold values from -0.125 to 0.125
- w_value: bfloat16 [2048, 1024], P(None, 'tp'), may hold values from -0.125 to 0.125
- w_outgate: bfloat16 [2048, 1024], P(None, 'tp'), may hold values from -0.125 to 0.125
- w_input_gate: bfloat16 [2048, 8], replicated, may hold values from -0.125 to 0.125
- w_forget_gate: bfloat16 [2048, 8], replicated, may hold values from -0.125 to 0.125
- forget_bias: float32 [8], replicated, may hold values from -1 to 4
- w_mix_out: bfloat16 [1024, 2048], P('tp')
- state_matrix: float32 [1024, 8, 128, 128], P('ep', 'tp'), may hold values from -0.6 to 0.6
- state_norm: float32 [1024, 8, 128], P('ep', 'tp'), may hold values from -0.6 to 0.6
- state_max: float32 [1024, 8], P('ep', 'tp'), may hold values from -4 to 4
- routes: int32 [1024, 2], P('ep'), may hold values from 0 to 31, all different within a row; in each aligned block of 32 rows (0 to 31, 32 to 63, ...) at most 4 rows name the same one
- route_scores: float32 [1024, 2], P('ep'), may hold values from 0.1 to 1
- expert_gate: bfloat16 [32, 2048, 3584], P('ep', None, 'tp'), may hold values from -0.125 to 0.125
- expert_up: bfloat16 [32, 2048, 3584], P('ep', None, 'tp'), may hold values from -0.125 to 0.125
- expert_down: bfloat16 [32, 3584, 2048], P('ep', 'tp')
- dense_gate: bfloat16 [2048, 5632], P('tp', 'ep'), may hold values from -0.125 to 0.125
- dense_up: bfloat16 [2048, 5632], P('tp', 'ep'), may hold values from -0.125 to 0.125
- dense_down: bfloat16 [5632, 2048], P('ep', 'tp')
- dense_mix: float32 [2048], replicated, may hold values from -0.25 to 0.25
Outputs:
- new_hidden: bfloat16 [1024, 2048], P('ep', 'tp')
- new_matrix: float32 [1024, 8, 128, 128], P('ep', 'tp')
- new_norm: float32 [1024, 8, 128], P('ep', 'tp')
- new_max: float32 [1024, 8], P('ep', 'tp')
Inputs may be any that keep to these rules, and one draw needn't show every extreme that they name: `routes`: each row names 2 different experts. Among the rows of one index of ep (an aligned block of 32 rows) no expert is named by more than 4 rows, and in every draw some expert is named by exactly 4 rows of some block.
All inputs are finite; a program needn't handle non-finite values.
Results may differ from a plain program's by a relative error of at most 0.02.
Values may be sent and summed in bfloat16 or wider, within the bound.
A program may use at most 128 MiB of HBM per device.

v0:
```python
import jax
import jax.numpy as jnp
from jax import lax
from jax.sharding import PartitionSpec as P

EPS = 1e-06


def split_up(x, dim, size):
    before, after = (x.shape[:dim], x.shape[dim + 1 :])
    return jnp.moveaxis(x.reshape(*before, size, -1, *after), dim, 0)


def sent_and_summed(x, axis, dim):
    size = lax.axis_size(axis)
    pieces = lax.all_to_all(split_up(x, dim, size), axis, 0, 0, tiled=True)
    return jnp.sum(pieces.astype(jnp.float32), axis=0)


def settle(values):
    return lax.optimization_barrier(values.astype(jnp.bfloat16)).astype(jnp.float32)


def local(
    hidden,
    norm_gains,
    w_query,
    w_key,
    w_value,
    w_outgate,
    w_input_gate,
    w_forget_gate,
    forget_bias,
    w_mix_out,
    state_matrix,
    state_norm,
    state_max,
    routes,
    route_scores,
    expert_gate,
    expert_up,
    expert_down,
    dense_gate,
    dense_up,
    dense_down,
    dense_mix,
):
    tp_count = lax.axis_size("tp")
    ep_count = lax.axis_size("ep")
    tp_place = lax.axis_index("tp")
    seq_local, width = hidden.shape
    heads_local = state_matrix.shape[1]
    head_width = state_matrix.shape[2]
    part_width = width // tp_count
    feature_first = tp_place * part_width
    start_f = hidden.astype(jnp.float32)
    normed_in = (
        start_f
        * lax.rsqrt(jnp.mean(start_f * start_f, axis=-1, keepdims=True) + EPS)
        * norm_gains[0]
    ).astype(jnp.bfloat16)
    query_f = jnp.dot(normed_in, w_query, preferred_element_type=jnp.float32)
    key_f = jnp.dot(normed_in, w_key, preferred_element_type=jnp.float32)
    value_f = jnp.dot(normed_in, w_value, preferred_element_type=jnp.float32)
    gate_f = jnp.dot(normed_in, w_outgate, preferred_element_type=jnp.float32)
    head_first = tp_place * heads_local
    input_weight = lax.dynamic_slice_in_dim(w_input_gate, head_first, heads_local, 1)
    forget_weight = lax.dynamic_slice_in_dim(w_forget_gate, head_first, heads_local, 1)
    forget_local = lax.dynamic_slice_in_dim(forget_bias, head_first, heads_local, 0)
    in_gate = jnp.dot(normed_in, input_weight, preferred_element_type=jnp.float32)
    log_forget = jax.nn.log_sigmoid(
        jnp.dot(normed_in, forget_weight, preferred_element_type=jnp.float32) + forget_local
    )
    query = settle(query_f).reshape(seq_local, heads_local, head_width)
    keys = settle(key_f).reshape(seq_local, heads_local, head_width) * head_width ** (-0.5)
    values = settle(value_f).reshape(seq_local, heads_local, head_width)
    carried = log_forget + state_max
    new_max = jnp.maximum(carried, in_gate)
    keep = jnp.exp(carried - new_max)
    write = jnp.exp(in_gate - new_max)
    written = write[:, :, None] * keys
    new_matrix = (
        keep[:, :, None, None] * state_matrix + written[:, :, :, None] * values[:, :, None, :]
    )
    new_norm = keep[:, :, None] * state_norm + written
    numer = jnp.einsum("shd,shdv->shv", query, new_matrix)
    denom = jnp.einsum("shd,shd->sh", query, new_norm)
    read = numer / jnp.maximum(jnp.abs(denom), jnp.exp(-new_max))[:, :, None]
    mixed = (
        jax.nn.sigmoid(settle(gate_f)) * read.reshape(seq_local, heads_local * head_width)
    ).astype(jnp.bfloat16)
    branch_terms = settle(jnp.dot(mixed, w_mix_out, preferred_element_type=jnp.float32))
    branch = settle(sent_and_summed(branch_terms.astype(jnp.bfloat16), "tp", 1))
    start_part = lax.dynamic_slice_in_dim(start_f, feature_first, part_width, 1)
    gain_rows = lax.dynamic_slice_in_dim(norm_gains, feature_first, part_width, 1)
    lifted = gain_rows[1] * branch
    mix_weight = gain_rows[2] * lax.dynamic_slice_in_dim(dense_mix, feature_first, part_width, 0)
    branch_sq, start_sq, cross_sum, lifted_sq, start_dot, lifted_dot = lax.psum(
        (
            jnp.sum(branch * branch, axis=-1),
            jnp.sum(start_part * start_part, axis=-1),
            jnp.sum(start_part * lifted, axis=-1),
            jnp.sum(lifted * lifted, axis=-1),
            jnp.sum(start_part * mix_weight, axis=-1),
            jnp.sum(lifted * mix_weight, axis=-1),
        ),
        "tp",
    )
    branch_scale = lax.rsqrt(branch_sq / width + EPS)
    residual_f = start_part + lifted * branch_scale[:, None]
    resid_sq = start_sq + 2.0 * branch_scale * cross_sum + branch_scale * branch_scale * lifted_sq
    gate_dot = start_dot + branch_scale * lifted_dot
    scale_two = lax.rsqrt(resid_sq / width + EPS)
    mix_gate = jax.nn.sigmoid(scale_two * gate_dot)
    residual = settle(residual_f)
    normed = (residual_f * scale_two[:, None] * gain_rows[2]).astype(jnp.bfloat16)
    rows_in = lax.all_gather(normed, "ep", axis=0, tiled=True)
    dense_pre = jnp.concatenate(
        [
            jnp.dot(rows_in, dense_gate, preferred_element_type=jnp.float32),
            jnp.dot(rows_in, dense_up, preferred_element_type=jnp.float32),
        ],
        axis=1,
    )
    dense_pre = lax.psum(dense_pre.astype(jnp.bfloat16), "tp").astype(jnp.float32)
    dense_pre_gate, dense_pre_up = jnp.split(dense_pre, 2, axis=1)
    dense_hidden = (jax.nn.silu(dense_pre_gate) * dense_pre_up).astype(jnp.bfloat16)
    dense_out = sent_and_summed(
        jnp.dot(dense_hidden, dense_down, preferred_element_type=jnp.float32).astype(jnp.bfloat16),
        "ep",
        0,
    )
    route_width = routes.shape[1]
    expert_count = ep_count * expert_gate.shape[0]
    capacity = 2 * seq_local * route_width // ep_count
    flat_expert = routes.reshape(-1)
    picks = (flat_expert[:, None] == jnp.arange(expert_count, dtype=jnp.int32)[None, :]).astype(
        jnp.int32
    )
    ranks = jnp.sum(jnp.cumsum(picks, axis=0) * picks, axis=1) - 1
    slot_index = flat_expert * capacity + ranks
    placing = (
        jnp.arange(expert_count * capacity, dtype=jnp.int32)[:, None] == slot_index[None, :]
    ).astype(jnp.bfloat16)
    repeated = jnp.repeat(normed, route_width, axis=0)
    outgoing = (
        jnp.dot(placing, repeated, preferred_element_type=jnp.float32)
        .astype(jnp.bfloat16)
        .reshape(expert_count, capacity, part_width)
    )
    arrived = lax.all_to_all(outgoing, "ep", split_axis=0, concat_axis=0, tiled=True)
    full_rows = lax.all_gather(arrived, "tp", axis=2, tiled=True)
    flat_rows = full_rows.reshape(-1, width)
    gate_pre = jnp.dot(flat_rows, expert_gate[0], preferred_element_type=jnp.float32)
    up_pre = jnp.dot(flat_rows, expert_up[0], preferred_element_type=jnp.float32)
    hidden_units = (jax.nn.silu(gate_pre) * up_pre).astype(jnp.bfloat16)
    partial_out = settle(jnp.dot(hidden_units, expert_down[0], preferred_element_type=jnp.float32))
    summed_out = sent_and_summed(partial_out.astype(jnp.bfloat16), "tp", 1).astype(jnp.bfloat16)
    returned = lax.all_to_all(
        summed_out.reshape(arrived.shape), "ep", split_axis=0, concat_axis=0, tiled=True
    )
    picked = lax.dot_general(
        placing,
        returned.reshape(expert_count * capacity, part_width),
        (((0,), (0,)), ((), ())),
        preferred_element_type=jnp.float32,
    )
    share = route_scores / jnp.sum(route_scores, axis=-1, keepdims=True)
    moe_out = jnp.sum(
        picked.reshape(seq_local, route_width, part_width) * share[:, :, None], axis=1
    )
    ffn = moe_out + mix_gate[:, None] * dense_out
    ffn_sq = lax.psum(jnp.sum(ffn * ffn, axis=-1), "tp")
    new_hidden = (residual + gain_rows[3] * ffn * lax.rsqrt(ffn_sq / width + EPS)[:, None]).astype(
        jnp.bfloat16
    )
    return (new_hidden, new_matrix, new_norm, new_max)


def solution(mesh):
    placed = (
        P("ep", None),
        P(),
        P(None, "tp"),
        P(None, "tp"),
        P(None, "tp"),
        P(None, "tp"),
        P(),
        P(),
        P(),
        P("tp", None),
        P("ep", "tp", None, None),
        P("ep", "tp", None),
        P("ep", "tp"),
        P("ep", None),
        P("ep", None),
        P("ep", None, "tp"),
        P("ep", None, "tp"),
        P("ep", "tp", None),
        P("tp", "ep"),
        P("tp", "ep"),
        P("ep", "tp"),
        P(),
    )
    return jax.shard_map(
        local,
        mesh=mesh,
        in_specs=placed,
        out_specs=(P("ep", "tp"), P("ep", "tp", None, None), P("ep", "tp", None), P("ep", "tp")),
        check_vma=False,
    )
```

profile of v0, /device:TPU:0, one launch (start us, length us, event | category | flops | bytes accessed | tf_op | source)
XLA Modules:
  0.0 185.0 jit_solution(4493191902834342916)
XLA Ops:
  7.2 0.9 slice.14
  8.1 1.0 multiply_reduce_fusion
  9.2 1.6 convolution_convert_fusion.7
  10.9 1.1 fusion.45
  12.0 0.7 dynamic_slice.21
  12.7 1.2 subtract_exponential_fusion
  14.1 1.6 convolution_convert_fusion.6
  15.8 1.6 convolution_convert_fusion.5
  17.4 0.8 fusion.39
  18.4 0.3 convolution_convert_fusion.8
  18.7 3.7 %multiply_add_fusion = f32[32,2,128,128]{3,2,1,0:T(8,128)S(1)} fusion(f32[32,2,128,128]{3,2,1,0:T(8,128)} %param.32, f32[32,2,128]{2,1,0:T(2,128)S(1)} %reshape.124, f32[32,2,128]{2,1,0:T(2,128)S(1)} %get-tuple-element.20, f32[32,2]{1,0:T(8,128)S(1)} %copy.37), kind=kLoop, calls=%fused_computation | loop fusion | flops 3145728 | bytes 8454400 | tf_op jit(solution)/shard_map/add | solution.py:83
  22.4 2.0 %copy-done.1 = f32[32,2,128,128]{3,2,1,0:T(8,128)} copy-done((f32[32,2,128,128]{3,2,1,0:T(8,128)}, f32[32,2,128,128]{3,2,1,0:T(8,128)S(1)}, u32[]{:S(2)}) %copy-start.1) | copy-done | bytes 4194328
  24.4 0.7 fusion.58
  25.1 0.1 broadcast_divide_fusion
  25.2 0.2 convolution_convert_fusion
  25.5 0.7 copy.62
  26.1 4.4 %all-to-all-start = ((bf16[4,32,512]{2,1,0:T(8,128)(2,1)}), bf16[4,32,512]{2,1,0:T(8,128)(2,1)S(1)}, u32[]{:S(2)}, u32[]{:S(2)}) async-start(bf16[4,32,512]{2,1,0:T(8,128)(2,1)} %bitcast.59), calls=%async_computation | async-start | bytes 262144 | tf_op jit(solution)/shard_map/all_to_all | solution.py:16
  30.5 0.9 fusion.57
  31.4 0.8 dynamic-slice_multiply_fusion
  32.2 4.3 %all-to-all-done = bf16[4,32,512]{2,1,0:T(8,128)(2,1)S(1)} async-done(((bf16[4,32,512]{2,1,0:T(8,128)(2,1)}), bf16[4,32,512]{2,1,0:T(8,128)(2,1)S(1)}, u32[]{:S(2)}, u32[]{:S(2)}) %all-to-all-start) | async-done | bytes 131104 | tf_op jit(solution)/shard_map/all_to_all | solution.py:16
  36.5 0.2 multiply_reduce_fusion.2
  36.7 8.9 %all-reduce = (f32[32]{0:T(128)S(1)}, f32[32]{0:T(128)S(1)}, f32[32]{0:T(128)S(1)}, f32[32]{0:T(128)S(1)}, f32[32]{0:T(128)S(1)}, /*index=5*/f32[32]{0:T(128)S(1)}) all-reduce(f32[32]{0:T(128)S(1)} %get-tuple-element.9, f32[32]{0:T(128)S(1)} %get-tuple-element.8, f32[32]{0:T(128)S(1)} %get-tuple-element.5, ...), channel_id=1, replica_groups=mesh['ep'=32,'tp'=4] {'tp'}, use_global_device_ids=true, to_apply=%region_3.4 | all-reduce | flops 192 | bytes 1536 | tf_op jit(solution)/shard_map/psum | solution.py:98
  45.7 0.7 multiply_convert_fusion.1
  46.8 0.2 select_reduce_fusion
  47.0 0.8 broadcast_in_dim.2
  47.9 0.2 convolution_convert_fusion.4
  48.1 16.1 %all_to_all.25 = bf16[32,4,512]{2,1,0:T(4,128)(2,1)S(1)} all-to-all(bf16[32,4,512]{2,1,0:T(4,128)(2,1)S(1)} %reshape.116), channel_id=1, replica_groups=mesh['ep'=32,'tp'=4] {'ep'}, dimensions={0} | all-to-all | bytes 262144 | tf_op jit(solution)/shard_map/all_to_all | solution.py:151
  64.2 13.4 %all_gather.6 = bf16[32,4,2048]{2,1,0:T(4,128)(2,1)S(1)} all-gather(bf16[32,4,512]{2,1,0:T(4,128)(2,1)S(1)} %all_to_all.25), channel_id=1, replica_groups=mesh['ep'=32,'tp'=4] {'tp'}, dimensions={2}, use_global_device_ids=true | all-gather | bytes 655360 | tf_op jit(solution)/shard_map/all_gather | solution.py:152
  77.6 0.1 reshape.117
  77.7 2.8 %fusion.4 = f32[128,896]{1,0:T(8,128)S(1)} fusion(bf16[128,2048]{1,0:T(8,128)(2,1)S(1)} %reshape.117, bf16[1,2048,896]{2,1,0:T(8,128)(2,1)} %param.37), kind=kOutput, calls=%fused_computation.5 | convolution fusion | flops 469762048 | bytes 4653056 | tf_op jit(solution)/shard_map/dot_general | solution.py:154
  80.5 9.0 %all-gather.2.cloned.1.call-done = bf16[1024,512]{1,0:T(8,128)(2,1)} async-done(((bf16[32,512]{1,0:T(8,128)(2,1)}), bf16[1024,512]{1,0:T(8,128)(2,1)}) %all-gather.2.cloned.1.call-update) | async-done | bytes 1048592 | tf_op jit(solution)/shard_map/all_gather | solution.py:117
  89.5 1.7 convolution_convert_fusion.2
  91.2 1.7 convolution_convert_fusion.3
  92.9 0.9 pad_maximum_fusion
  93.9 4.5 %fusion.6 = bf16[128,2048]{1,0:T(8,128)(2,1)S(1)} fusion(bf16[1,896,2048]{2,1,0:T(8,128)(2,1)} %param.39, bf16[128,2048]{1,0:T(8,128)(2,1)S(1)} %reshape.117, bf16[1,2048,896]{2,1,0:T(8,128)(2,1)} %param.38, f32[128,896]{1,0:T(8,128)S(1)} %fusion.4), kind=kOutput, calls=%fused_computation.7 | convolution fusion | flops 940474368 | bytes 8847360 | tf_op jit(solution)/shard_map/dot_general | solution.py:157
  98.5 17.7 %all_to_all.26 = bf16[4,128,512]{2,1,0:T(8,128)(2,1)S(1)} all-to-all(bf16[4,128,512]{2,1,0:T(8,128)(2,1)S(1)} %bitcast.60), channel_id=1, replica_groups=mesh['ep'=32,'tp'=4] {'tp'}, dimensions={0} | all-to-all | bytes 1048576 | tf_op jit(solution)/shard_map/all_to_all | solution.py:16
  116.2 0.7 reshape.119
  116.9 6.5 %all-to-all-start.3 = ((bf16[32,4,512]{2,1,0:T(4,128)(2,1)}), bf16[32,4,512]{2,1,0:T(4,128)(2,1)S(1)}, u32[]{:S(2)}, u32[]{:S(2)}) async-start(bf16[32,4,512]{2,1,0:T(4,128)(2,1)} %reshape.119), calls=%async_computation.3 | async-start | bytes 262144 | tf_op jit(solution)/shard_map/all_to_all | solution.py:159
  123.4 17.0 %all-reduce.3.cloned.1.call-done = bf16[1024,352]{0,1:T(8,128)(2,1)} async-done(((bf16[1024,352]{0,1:T(8,128)(2,1)}), bf16[1024,352]{0,1:T(8,128)(2,1)}) %all-reduce.3.cloned.1.call-update) | async-done | bytes 720912 | tf_op jit(solution)/shard_map/psum | solution.py:125
  140.4 1.3 convert_element_type.96
  141.7 1.5 convolution_convert_fusion.1
  143.2 7.3 %all-to-all-start.4 = ((bf16[32,32,512]{2,1,0:T(8,128)(2,1)}), bf16[32,32,512]{2,1,0:T(8,128)(2,1)S(1)}, u32[]{:S(2)}, u32[]{:S(2)}) async-start(bf16[32,32,512]{2,1,0:T(8,128)(2,1)} %bitcast.11), calls=%async_computation.4 | async-start | bytes 2097152 | tf_op jit(solution)/shard_map/all_to_all | solution.py:16
  150.7 0.2 fusion.15
  150.8 16.9 %all-to-all-done.4 = bf16[32,32,512]{2,1,0:T(8,128)(2,1)S(1)} async-done(((bf16[32,32,512]{2,1,0:T(8,128)(2,1)}), bf16[32,32,512]{2,1,0:T(8,128)(2,1)S(1)}, u32[]{:S(2)}, u32[]{:S(2)}) %all-to-all-start.4) | async-done | bytes 1048608 | tf_op jit(solution)/shard_map/all_to_all | solution.py:16
  167.7 0.2 convert_reduce_fusion
  167.9 0.2 multiply_reduce_fusion.1
  168.0 9.4 %psum.63 = f32[32]{0:T(128)S(1)} all-reduce(f32[32]{0:T(128)S(1)} %multiply_reduce_fusion.1), channel_id=1, replica_groups=mesh['ep'=32,'tp'=4] {'tp'}, use_global_device_ids=true, to_apply=%region_22.23 | all-reduce | flops 32 | bytes 256 | tf_op jit(solution)/shard_map/psum | solution.py:173
  177.4 0.7 add_convert_fusion
  (55 shorter events, 1.4 us)
Async XLA Ops:
  7.2 18.0 %copy-start = (bf16[256,2048]{1,0:T(8,128)(2,1)S(1)}, bf16[256,2048]{1,0:T(8,128)(2,1)}, u32[]{:S(2)}) copy-start(bf16[256,2048]{1,0:T(8,128)(2,1)} %param.31) | copy-start | bytes 3145732
  7.2 11.2 %copy-start.2 = (bf16[32,2048]{1,0:T(8,128)(2,1)S(1)}, bf16[32,2048]{1,0:T(8,128)(2,1)}, u32[]{:S(2)}) copy-start(bf16[32,2048]{1,0:T(8,128)(2,1)} %param.22) | copy-start | bytes 393220
  7.2 10.2 %copy-start.6 = (f32[32,2,128]{2,1,0:T(2,128)S(1)}, f32[32,2,128]{2,1,0:T(2,128)}, u32[]{:S(2)}) copy-start(f32[32,2,128]{2,1,0:T(2,128)} %param.33) | copy-start | bytes 98308
  7.2 11.2 %copy-start.3 = (bf16[2048,256]{1,0:T(8,128)(2,1)S(1)}, bf16[2048,256]{1,0:T(8,128)(2,1)}, u32[]{:S(2)}) copy-start(bf16[2048,256]{1,0:T(8,128)(2,1)} %param.27) | copy-start | bytes 3145732
  13.9 8.5 %copy-start.7 = (f32[32,2]{0,1:T(2,128)}, f32[32,2]{0,1:T(2,128)S(1)}, u32[]{:S(2)}) copy-start(f32[32,2]{0,1:T(2,128)S(1)} %get-tuple-element.22) | copy-start | bytes 772
  22.4 2.0 %copy-start.1 = (f32[32,2,128,128]{3,2,1,0:T(8,128)}, f32[32,2,128,128]{3,2,1,0:T(8,128)S(1)}, u32[]{:S(2)}) copy-start(f32[32,2,128,128]{3,2,1,0:T(8,128)S(1)} %multiply_add_fusion) | copy-start | bytes 12582916
  24.4 22.0 %copy-start.9 = (s32[32,2]{0,1:T(2,128)S(1)}, s32[32,2]{0,1:T(2,128)}, u32[]{:S(2)}) copy-start(s32[32,2]{0,1:T(2,128)} %param.35) | copy-start | bytes 772
  26.1 10.4 %all-to-all-start = ((bf16[4,32,512]{2,1,0:T(8,128)(2,1)}), bf16[4,32,512]{2,1,0:T(8,128)(2,1)S(1)}, u32[]{:S(2)}, u32[]{:S(2)}) async-start(bf16[4,32,512]{2,1,0:T(8,128)(2,1)} %bitcast.59), calls=%async_computation | async-start | bytes 262144 | tf_op jit(solution)/shard_map/all_to_all | solution.py:16
  30.5 59.0 %all-gather.2.cloned.1.call-start = ((), (), s32[]{:S(2)}) async-start(), calls=%async_computation.5 | async-start | bytes 1081344 | tf_op jit(solution)/shard_map/all_gather | solution.py:117
  46.4 94.0 %all-reduce.3.cloned.1.call-start = ((), (), s32[]{:S(2)}) async-start(), calls=%async_computation.6 | async-start | bytes 1441792 | tf_op jit(solution)/shard_map/psum | solution.py:125
  46.8 42.7 %copy-start.4 = (bf16[512,176]{0,1:T(8,128)(2,1)S(1)}, bf16[512,176]{0,1:T(8,128)(2,1)}, u32[]{:S(2)}) copy-start(bf16[512,176]{0,1:T(8,128)(2,1)} %param.41) | copy-start | bytes 540676
  77.6 13.6 %copy-start.5 = (bf16[512,176]{0,1:T(8,128)(2,1)S(1)}, bf16[512,176]{0,1:T(8,128)(2,1)}, u32[]{:S(2)}) copy-start(bf16[512,176]{0,1:T(8,128)(2,1)} %param.40) | copy-start | bytes 540676
  98.4 43.3 %copy-start.10 = (bf16[176,512]{1,0:T(8,128)(2,1)S(1)}, bf16[176,512]{1,0:T(8,128)(2,1)}, u32[]{:S(2)}) copy-start(bf16[176,512]{1,0:T(8,128)(2,1)} %param.42) | copy-start | bytes 540676
  116.9 26.3 %all-to-all-start.3 = ((bf16[32,4,512]{2,1,0:T(4,128)(2,1)}), bf16[32,4,512]{2,1,0:T(4,128)(2,1)S(1)}, u32[]{:S(2)}, u32[]{:S(2)}) async-start(bf16[32,4,512]{2,1,0:T(4,128)(2,1)} %reshape.119), calls=%async_computation.3 | async-start | bytes 262144 | tf_op jit(solution)/shard_map/all_to_all | solution.py:159
  141.7 8.9 %copy-start.8 = (f32[32,2]{0,1:T(2,128)S(1)}, f32[32,2]{0,1:T(2,128)}, u32[]{:S(2)}) copy-start(f32[32,2]{0,1:T(2,128)} %param.36) | copy-start | bytes 772
  143.2 24.5 %all-to-all-start.4 = ((bf16[32,32,512]{2,1,0:T(8,128)(2,1)}), bf16[32,32,512]{2,1,0:T(8,128)(2,1)S(1)}, u32[]{:S(2)}, u32[]{:S(2)}) async-start(bf16[32,32,512]{2,1,0:T(8,128)(2,1)} %bitcast.11), calls=%async_computation.4 | async-start | bytes 2097152 | tf_op jit(solution)/shard_map/all_to_all | solution.py:16
Sparse Core Ops, SparseCore 0:
  46.5 42.9 all-gather.1
  94.0 46.3 all-reduce.2
where the time goes:
time: 186 us; the launch traced here: 185 us
  blocking collectives  65.5 us (35%)
  waiting for transfers between devices  47.2 us (25%)
  matrix products  21 us (11%)
  starting transfers between devices  18.2 us (10%)
  between operations  14.4 us (8%)
  other arithmetic  11.1 us (6%)
  local copies, waits for them, and re-layouts  7.66 us (4%)
    all_to_all x2, waiting for transfers between devices, sent_and_summed(): pieces = lax.all_to_all(split_up(x, dim, size), axis, 0, 0, tiled=True)  21.2 us
    all_to_all x1, blocking collectives, sent_and_summed(): pieces = lax.all_to_all(split_up(x, dim, size), axis, 0, 0, tiled=True)  17.7 us
    psum x1, waiting for transfers between devices, local(): lax.psum(dense_pre.astype(jnp.bfloat16), 'tp').astype(jnp.float32)  17 us
    all_to_all x1, blocking collectives, local(): lax.all_to_all(outgoing, 'ep', split_axis=0, concat_axis=0, tiled=True)  16.1 us
    all_gather x1, blocking collectives, local(): full_rows = lax.all_gather(arrived, 'tp', axis=2, tiled=True)  13.4 us
    all_to_all x2, starting transfers between devices, sent_and_summed(): pieces = lax.all_to_all(split_up(x, dim, size), axis, 0, 0, tiled=True)  11.7 us
    psum x1, blocking collectives, local(): ffn_sq = lax.psum(jnp.sum(ffn * ffn, axis=-1), 'tp')  9.37 us
    all_gather x1, waiting for transfers between devices, local(): rows_in = lax.all_gather(normed, 'ep', axis=0, tiled=True)  8.99 us
  transfers between devices with their start and end apart: 5, of which 4 were waited for; matrix products, arithmetic and copies ran while one was open for 8% of the time, Pallas kernels for 0%

commit v1 on v0

v1 whole, which is shorter than its diff:
```python
import functools

import jax
import jax.numpy as jnp
from jax import lax
from jax.experimental import pallas as pl
from jax.experimental.pallas import tpu as pltpu
from jax.sharding import PartitionSpec as P

EPS = 1e-06
MESH = pl.DeviceIdType.MESH
BF = jnp.bfloat16
F32 = jnp.float32
I32 = jnp.int32
CH = 512


def dot(a, b):
    return jnp.dot(a, b, preferred_element_type=F32)


def iota(shape, dim):
    return lax.broadcasted_iota(I32, shape, dim)


def one_hot(columns, rows, target):
    return (iota((rows, columns), 1) == target(iota((rows, columns), 0))).astype(BF)


def stacked(ref):
    return jnp.concatenate([ref[:, q * CH : (q + 1) * CH] for q in range(4)], axis=0)


def row_total(values):
    part = jnp.sum(values, axis=1, keepdims=True)
    total = part[0:8] + part[8:16] + part[16:24] + part[24:32]
    return jnp.concatenate([total] * 4, axis=0)


def silu(t):
    return t / (1.0 + jnp.exp(-t))


def rest_kernel(
    terms, hidden, gains, mix, routes, scores, eg, eu, ed, dg, du, dd,
    out,
    wg, wu, wd, dgv, duv, gbuf, dbuf,
    bsend, brecv, hperm, nall, tok, osend, orecv, rsend, rrecv, dsend, drecv,
    msend, mrecv, fsend, frecv,
    pm, pmi, pd, pdi, gk, xs, xd, ys, yd, hexp, hden, resid_s, mixg_s, share_s,
    load_sem, b_sem, n_sem, t_sem, o_sem, r_sem, d_sem, m_sem, f_sem,
    gs_sem, gr_sem, ds_sem, dr_sem,
):
    x = lax.axis_index("tp")
    ep = lax.axis_index("ep")
    c = ep % 2
    y = (ep // 2) % 4
    z = ep // 8
    p = ep // 2
    mate = p * 2 + (1 - c)
    left, right, far = (x + 3) % 4, (x + 1) % 4, (x + 2) % 4

    def plane(k):
        return ((z + k // 8) % 4) * 8 + ((y + (k // 2) % 4) % 4) * 2 + (c + k % 2) % 2

    def remote(src, dst, ssem, rsem, to_ep, to_x):
        return pltpu.make_async_remote_copy(
            src_ref=src, dst_ref=dst, send_sem=ssem, recv_sem=rsem,
            device_id=(to_ep, to_x), device_id_type=MESH,
        )

    def landed(ref, sem):
        pltpu.make_async_copy(ref, ref, sem).wait()

    barrier = pltpu.get_barrier_semaphore()

    def greet(k, carry):
        pl.semaphore_signal(barrier, inc=1, device_id=(plane(k), x), device_id_type=MESH)
        return carry

    for d in (2, 1, 3):
        pl.semaphore_signal(barrier, inc=1, device_id=(ep, (x + d) % 4), device_id_type=MESH)
    lax.fori_loop(1, 32, greet, 0)

    loads = [
        pltpu.make_async_copy(src, dst, load_sem.at[n])
        for n, (src, dst) in enumerate(
            [(dg, dgv), (du, duv), (dd, dbuf.at[c, x]), (eg, wg), (eu, wu), (ed, wd)]
        )
    ]
    for load in loads:
        load.start()

    order = one_hot(128, 128, lambda r: ((r >> 3) & 3) * 32 + (r >> 5) * 8 + (r & 7))
    bsend[...] = dot(order, stacked(terms)).astype(BF).reshape(4, 32, CH)
    brecv[x] = bsend[x]
    pl.semaphore_wait(barrier, 34)
    branch_out = []
    for d in (2, 1, 3):
        to = (x + d) % 4
        branch_out.append(remote(bsend.at[to], brecv.at[x], b_sem.at[0], b_sem.at[1], ep, to))
        branch_out[-1].start()

    hperm[...] = dot(order, stacked(hidden)).reshape(4, 32, CH)

    expert0, expert1 = routes[:, 0:1], routes[:, 1:2]
    lane32 = iota((32, 32), 1)
    hot0 = (lane32 == expert0).astype(F32)
    hot1 = (lane32 == expert1).astype(F32)
    earlier = (iota((32, 32), 0) > lane32).astype(BF)
    before = dot(earlier, (hot0 + hot1).astype(BF))
    score0, score1 = scores[:, 0:1], scores[:, 1:2]
    whole = score0 + score1

    def by_piece(column, step):
        return jnp.concatenate(
            [column[xx * 8 : xx * 8 + 8] + q * step for xx in range(4) for q in range(4)], axis=0
        )

    for k, (expert, hot, score) in enumerate(((expert0, hot0, score0), (expert1, hot1, score1))):
        rank = jnp.sum(hot * before, axis=1, keepdims=True).astype(I32)
        place = by_piece(expert * 16 + rank, 4)
        gk[k] = (iota((128, 512), 1) == place).astype(BF)
        share_s[k] = jnp.broadcast_to(by_piece(score / whole, 0.0), (128, 128))
    pm[...] = one_hot(512, 512, lambda r: ((r >> 2) & 31) * 16 + (r >> 7) * 4 + (r & 3))
    pmi[...] = one_hot(512, 512, lambda r: ((r >> 2) & 3) * 128 + (r >> 4) * 4 + (r & 3))
    pd[...] = one_hot(512, 512, lambda r: ((r >> 3) & 15) * 32 + (r >> 7) * 8 + (r & 7))
    pdi[...] = one_hot(512, 512, lambda r: ((r >> 3) & 3) * 128 + (r >> 5) * 8 + (r & 7))

    def gain(k):
        return jnp.concatenate(
            [jnp.broadcast_to(gains[k : k + 1, q * CH : (q + 1) * CH], (8, CH)) for q in range(4)],
            axis=0,
        )

    mix_rows = jnp.concatenate(
        [jnp.broadcast_to(mix[0:1, q * CH : (q + 1) * CH], (8, CH)) for q in range(4)], axis=0
    )

    landed(brecv.at[pl.ds(0, 3)], b_sem.at[1])
    branch = brecv[0].astype(F32) + brecv[1].astype(F32) + brecv[2].astype(F32) + brecv[3].astype(F32)
    branch = branch.astype(BF).astype(F32)
    residual_f = hperm[x] + gain(1) * branch * lax.rsqrt(row_total(branch * branch) / 2048.0 + EPS)
    scale_two = lax.rsqrt(row_total(residual_f * residual_f) / 2048.0 + EPS)
    normed = (residual_f * scale_two * gain(2)).astype(BF)
    nall[x] = normed
    tok[p] = normed

    token_out = []
    for d in (2, 1, 3):
        to = (x + d) % 4
        token_out.append(remote(nall.at[x], nall.at[x], n_sem.at[0], n_sem.at[1], ep, to))
        token_out[-1].start()

    def share_tokens(k, carry):
        to = ((z + k // 4) % 4) * 8 + ((y + k % 4) % 4) * 2 + c
        remote(nall.at[x], tok.at[p], t_sem.at[0], t_sem.at[1], to, x).start()
        return carry

    resid_s[...] = residual_f.astype(BF).astype(F32)
    mix_dot = scale_two * row_total(residual_f * gain(2) * mix_rows)
    mixg_s[...] = jnp.broadcast_to(1.0 / (1.0 + jnp.exp(-mix_dot)), (32, 128))

    landed(nall.at[pl.ds(0, 3)], n_sem.at[1])
    chosen = gk[0] + gk[1]
    rows = lax.dot_general(
        chosen, nall[...].reshape(128, CH), (((0,), (0,)), ((), ())), preferred_element_type=F32
    )
    osend[...] = rows.astype(BF).reshape(32, 16, CH)
    orecv[ep] = osend[ep]

    def dispatch(k, carry):
        to = plane(k)
        remote(osend.at[to], orecv.at[ep], o_sem.at[0], o_sem.at[1], to, x).start()
        return carry

    lax.fori_loop(1, 32, dispatch, 0)
    lax.fori_loop(1, 16, share_tokens, 0)

    loads[0].wait()
    loads[1].wait()
    r176, l384 = iota((176, 384), 0), iota((176, 384), 1)
    into_gate = (l384 == jnp.where(r176 < 128, r176, r176 + 128)).astype(BF)
    into_up = (l384 == jnp.where(r176 < 128, r176 + 128, r176 + 192)).astype(BF)
    gbuf[c, x] = (dot(dgv[...], into_gate) + dot(duv[...], into_up)).astype(BF)
    loads[2].wait()

    def first_round(buf, ssem, rsem):
        block = buf.at[c, x]
        copies = [
            remote(block, block, ssem.at[0], rsem.at[0], ep, right),
            remote(block, block, ssem.at[1], rsem.at[1], ep, left),
            remote(block, block, ssem.at[4], rsem.at[4], mate, x),
        ]
        for copy in copies:
            copy.start()
        return copies

    def second_round(buf, cut, ssem, rsem):
        size = buf.shape[2]
        from_left, from_right = buf.at[c, left], buf.at[c, right]
        low = buf.at[c, left, pl.ds(0, cut)]
        high = buf.at[c, right, pl.ds(cut, size - cut)]
        copies = [
            remote(low, low, ssem.at[2], rsem.at[2], ep, right),
            remote(from_left, from_left, ssem.at[5], rsem.at[5], mate, x),
            remote(high, high, ssem.at[3], rsem.at[3], ep, left),
            remote(from_right, from_right, ssem.at[6], rsem.at[6], mate, x),
        ]
        landed(from_left, rsem.at[0])
        copies[0].start()
        copies[1].start()
        landed(from_right, rsem.at[1])
        copies[2].start()
        copies[3].start()
        return copies

    def third_round(buf, cut, ssem, rsem):
        size = buf.shape[2]
        block = buf.at[c, far]
        landed(buf.at[c, far, pl.ds(0, cut)], rsem.at[2])
        landed(buf.at[c, far, pl.ds(cut, size - cut)], rsem.at[3])
        copy = remote(block, block, ssem.at[7], rsem.at[7], mate, x)
        copy.start()
        return [copy]

    def from_mate(buf, rsem):
        for n, place in ((4, x), (5, left), (6, right), (7, far)):
            landed(buf.at[1 - c, place], rsem.at[n])

    weight_out = first_round(gbuf, gs_sem, gr_sem) + first_round(dbuf, ds_sem, dr_sem)
    weight_out += second_round(gbuf, 256, gs_sem, gr_sem)

    landed(orecv.at[pl.ds(0, 31)], o_sem.at[1])
    xs[...] = dot(pm[...], orecv[...].reshape(512, CH)).astype(BF).reshape(4, 128, CH)
    loads[3].wait()
    loads[4].wait()
    gate_pre = dot(xs[0], wg[0])
    up_pre = dot(xs[0], wu[0])
    for q in range(1, 4):
        gate_pre += dot(xs[q], wg[q])
        up_pre += dot(xs[q], wu[q])
    hexp[...] = (silu(gate_pre) * up_pre).astype(BF)
    loads[5].wait()
    for q in range(4):
        ys[q * 128 : (q + 1) * 128] = dot(hexp[...], wd[:, q * CH : (q + 1) * CH]).astype(BF)
    rsend[...] = dot(pmi[...], ys[...]).astype(BF).reshape(32, 16, CH)
    rrecv[ep] = rsend[ep]

    def give_back(k, carry):
        to = plane(k)
        remote(rsend.at[to], rrecv.at[ep], r_sem.at[0], r_sem.at[1], to, x).start()
        return carry

    lax.fori_loop(1, 32, give_back, 0)

    weight_out += third_round(gbuf, 256, gs_sem, gr_sem)
    weight_out += second_round(dbuf, 96, ds_sem, dr_sem)

    landed(tok.at[pl.ds(0, 15)], t_sem.at[1])
    xd[...] = dot(pd[...], tok[...].reshape(512, CH)).astype(BF).reshape(4, 128, CH)
    from_mate(gbuf, gr_sem)
    for core in range(2):
        pre = dot(xd[0], gbuf[core, 0])
        for q in range(1, 4):
            pre += dot(xd[q], gbuf[core, q])
        tail = pre[:, 256:384]
        hden[core, :, 0:128] = (silu(pre[:, 0:128]) * pre[:, 128:256]).astype(BF)
        hden[core, :, 128:256] = (silu(tail) * pltpu.roll(tail, 64, 1)).astype(BF)
    weight_out += third_round(dbuf, 96, ds_sem, dr_sem)
    from_mate(dbuf, dr_sem)
    for q in range(4):
        yd[q * 128 : (q + 1) * 128] = (
            dot(hden[0, :, 0:176], dbuf[0, q]) + dot(hden[1, :, 0:176], dbuf[1, q])
        ).astype(BF)
    dsend[...] = dot(pdi[...], yd[...]).astype(BF).reshape(16, 32, CH)
    drecv[p] = dsend[p]

    def dense_back(k, carry):
        to = ((z + k // 4) % 4) * 4 + (y + k % 4) % 4
        remote(dsend.at[to], drecv.at[p], d_sem.at[0], d_sem.at[1], to * 2 + c, x).start()
        return carry

    lax.fori_loop(1, 16, dense_back, 0)

    landed(rrecv.at[pl.ds(0, 31)], r_sem.at[1])
    back = rrecv[...].reshape(512, CH)
    moe = share_s[0][:, 0:1] * dot(gk[0], back) + share_s[1][:, 0:1] * dot(gk[1], back)
    msend[...] = moe.astype(BF).reshape(4, 32, CH)
    mrecv[x] = msend[x]
    moe_out = []
    for d in (2, 1, 3):
        to = (x + d) % 4
        moe_out.append(remote(msend.at[to], mrecv.at[x], m_sem.at[0], m_sem.at[1], ep, to))
        moe_out[-1].start()

    landed(drecv.at[pl.ds(0, 15)], d_sem.at[1])
    dense = drecv[0].astype(F32)
    for n in range(1, 16):
        dense += drecv[n].astype(F32)
    landed(mrecv.at[pl.ds(0, 3)], m_sem.at[1])
    ffn = mrecv[0].astype(F32) + mrecv[1].astype(F32) + mrecv[2].astype(F32) + mrecv[3].astype(F32)
    ffn += mixg_s[:, 0:1] * dense
    scale_ffn = lax.rsqrt(row_total(ffn * ffn) / 2048.0 + EPS)
    fsend[...] = (resid_s[...] + gain(3) * ffn * scale_ffn).reshape(4, 8, CH)
    frecv[x] = fsend[x]
    last_out = []
    for d in (2, 1, 3):
        to = (x + d) % 4
        last_out.append(remote(fsend.at[to], frecv.at[x], f_sem.at[0], f_sem.at[1], ep, to))
        last_out[-1].start()

    for copy in weight_out:
        copy.wait_send()
    landed(bsend.at[pl.ds(0, 3)], b_sem.at[0])
    landed(nall.at[pl.ds(0, 3)], n_sem.at[0])
    landed(tok.at[pl.ds(0, 15)], t_sem.at[0])
    landed(osend.at[pl.ds(0, 31)], o_sem.at[0])
    landed(rsend.at[pl.ds(0, 31)], r_sem.at[0])
    landed(dsend.at[pl.ds(0, 15)], d_sem.at[0])
    landed(msend.at[pl.ds(0, 3)], m_sem.at[0])
    landed(frecv.at[pl.ds(0, 3)], f_sem.at[1])
    out[...] = frecv[...].reshape(32, CH).astype(BF)
    landed(fsend.at[pl.ds(0, 3)], f_sem.at[0])


def rest(terms, hidden, gains, mix, routes, scores, eg, eu, ed, dg, du, dd):
    V = pltpu.VMEM
    dma = pltpu.SemaphoreType.DMA
    vm = pl.BlockSpec(memory_space=pltpu.VMEM)
    hb = pl.BlockSpec(memory_space=pl.ANY)
    return pl.pallas_call(
        rest_kernel,
        out_shape=jax.ShapeDtypeStruct((32, CH), BF),
        in_specs=[vm] * 6 + [hb] * 6,
        out_specs=vm,
        scratch_shapes=[
            V((4, 512, 896), BF), V((4, 512, 896), BF), V((896, 2048), BF),
            V((512, 176), BF), V((512, 176), BF), V((2, 4, 512, 384), BF), V((2, 4, 176, 512), BF),
            V((4, 32, CH), BF), V((4, 32, CH), BF), V((4, 32, CH), F32), V((4, 32, CH), BF),
            V((16, 32, CH), BF),
            V((32, 16, CH), BF), V((32, 16, CH), BF), V((32, 16, CH), BF), V((32, 16, CH), BF),
            V((16, 32, CH), BF), V((16, 32, CH), BF),
            V((4, 32, CH), BF), V((4, 32, CH), BF), V((4, 8, CH), F32), V((4, 8, CH), F32),
            V((512, 512), BF), V((512, 512), BF), V((512, 512), BF), V((512, 512), BF),
            V((2, 128, 512), BF), V((4, 128, CH), BF), V((4, 128, CH), BF),
            V((512, CH), BF), V((512, CH), BF), V((128, 896), BF), V((2, 128, 256), BF),
            V((32, CH), F32), V((32, 128), F32), V((2, 128, 128), F32),
            dma((6,)), dma((2,)), dma((2,)), dma((2,)), dma((2,)), dma((2,)), dma((2,)),
            dma((2,)), dma((2,)), dma((8,)), dma((8,)), dma((8,)), dma((8,)),
        ],
        compiler_params=pltpu.CompilerParams(
            collective_id=0, has_side_effects=True, vmem_limit_bytes=60 * 1024 * 1024
        ),
        name="rest",
    )(terms, hidden, gains, mix, routes, scores, eg, eu, ed, dg, du, dd)


def settle(values):
    return lax.optimization_barrier(values.astype(jnp.bfloat16)).astype(jnp.float32)


def local(
    hidden,
    norm_gains,
    w_query,
    w_key,
    w_value,
    w_outgate,
    w_input_gate,
    w_forget_gate,
    forget_bias,
    w_mix_out,
    state_matrix,
    state_norm,
    state_max,
    routes,
    route_scores,
    expert_gate,
    expert_up,
    expert_down,
    dense_gate,
    dense_up,
    dense_down,
    dense_mix,
):
    tp_place = lax.axis_index("tp")
    seq_local, width = hidden.shape
    heads_local = state_matrix.shape[1]
    head_width = state_matrix.shape[2]
    start_f = hidden.astype(jnp.float32)
    normed_in = (
        start_f
        * lax.rsqrt(jnp.mean(start_f * start_f, axis=-1, keepdims=True) + EPS)
        * norm_gains[0]
    ).astype(jnp.bfloat16)
    query_f = jnp.dot(normed_in, w_query, preferred_element_type=jnp.float32)
    key_f = jnp.dot(normed_in, w_key, preferred_element_type=jnp.float32)
    value_f = jnp.dot(normed_in, w_value, preferred_element_type=jnp.float32)
    gate_f = jnp.dot(normed_in, w_outgate, preferred_element_type=jnp.float32)
    head_first = tp_place * heads_local
    input_weight = lax.dynamic_slice_in_dim(w_input_gate, head_first, heads_local, 1)
    forget_weight = lax.dynamic_slice_in_dim(w_forget_gate, head_first, heads_local, 1)
    forget_local = lax.dynamic_slice_in_dim(forget_bias, head_first, heads_local, 0)
    in_gate = jnp.dot(normed_in, input_weight, preferred_element_type=jnp.float32)
    log_forget = jax.nn.log_sigmoid(
        jnp.dot(normed_in, forget_weight, preferred_element_type=jnp.float32) + forget_local
    )
    query = settle(query_f).reshape(seq_local, heads_local, head_width)
    keys = settle(key_f).reshape(seq_local, heads_local, head_width) * head_width ** (-0.5)
    values = settle(value_f).reshape(seq_local, heads_local, head_width)
    carried = log_forget + state_max
    new_max = jnp.maximum(carried, in_gate)
    keep = jnp.exp(carried - new_max)
    write = jnp.exp(in_gate - new_max)
    written = write[:, :, None] * keys
    new_matrix = (
        keep[:, :, None, None] * state_matrix + written[:, :, :, None] * values[:, :, None, :]
    )
    new_norm = keep[:, :, None] * state_norm + written
    numer = jnp.einsum("shd,shdv->shv", query, new_matrix)
    denom = jnp.einsum("shd,shd->sh", query, new_norm)
    read = numer / jnp.maximum(jnp.abs(denom), jnp.exp(-new_max))[:, :, None]
    mixed = (
        jax.nn.sigmoid(settle(gate_f)) * read.reshape(seq_local, heads_local * head_width)
    ).astype(jnp.bfloat16)
    branch_terms = settle(jnp.dot(mixed, w_mix_out, preferred_element_type=jnp.float32))
    new_hidden = rest(
        branch_terms.astype(jnp.bfloat16),
        hidden,
        norm_gains,
        dense_mix.reshape(1, -1),
        routes,
        route_scores,
        expert_gate.reshape(4, CH, -1),
        expert_up.reshape(4, CH, -1),
        expert_down[0],
        dense_gate,
        dense_up,
        dense_down,
    )
    return (new_hidden, new_matrix, new_norm, new_max)


def solution(mesh):
    placed = (
        P("ep", None),
        P(),
        P(None, "tp"),
        P(None, "tp"),
        P(None, "tp"),
        P(None, "tp"),
        P(),
        P(),
        P(),
        P("tp", None),
        P("ep", "tp", None, None),
        P("ep", "tp", None),
        P("ep", "tp"),
        P("ep", None),
        P("ep", None),
        P("ep", None, "tp"),
        P("ep", None, "tp"),
        P("ep", "tp", None),
        P("tp", "ep"),
        P("tp", "ep"),
        P("ep", "tp"),
        P(),
    )
    return jax.shard_map(
        local,
        mesh=mesh,
        in_specs=placed,
        out_specs=(P("ep", "tp"), P("ep", "tp", None, None), P("ep", "tp", None), P("ep", "tp")),
        check_vma=False,
    )
```

time: 186 us -> 82 us (0.44)
  blocking collectives: 65.5 us -> 0 us
  Pallas kernels: 0 us -> 55.4 us
  waiting for transfers between devices: 47.2 us -> 0 us
  starting transfers between devices: 18.2 us -> 0 us
  between operations: 14.4 us -> 0.78 us
  matrix products: 21 us -> 11.4 us
  other arithmetic: 11.1 us -> 7.04 us
    pallas_call x0 -> x1, Pallas kernels: none -> 55.4 us  [rest(): pl.pallas_call(rest_kernel, out_shape=jax.ShapeDtypeStruct((32, CH), BF),...]
    all_to_all x2 -> x0, blocking collectives: 33.8 us -> none  [the longest x1 17.7 us: sent_and_summed(): pieces = lax.all_to_all(split_up(x, dim, size), axis, 0, 0, tiled=True)]
    all_to_all x3 -> x0, waiting for transfers between devices: 21.2 us -> none  [the longest x2 21.2 us: sent_and_summed(): pieces = lax.all_to_all(split_up(x, dim, size), axis, 0, 0, tiled=True)]
    psum x2 -> x0, blocking collectives: 18.3 us -> none  [the longest x1 9.37 us: local(): ffn_sq = lax.psum(jnp.sum(ffn * ffn, axis=-1), 'tp')]
    all_to_all x3 -> x0, starting transfers between devices: 18.1 us -> none  [the longest x2 11.7 us: sent_and_summed(): pieces = lax.all_to_all(split_up(x, dim, size), axis, 0, 0, tiled=True)]
    psum x1 -> x0, waiting for transfers between devices: 17 us -> none  [local(): lax.psum(dense_pre.astype(jnp.bfloat16), 'tp').astype(jnp.float32)]
    all_gather x1 -> x0, blocking collectives: 13.4 us -> none  [local(): full_rows = lax.all_gather(arrived, 'tp', axis=2, tiled=True)]
    dot_general x7 -> x0, matrix products: 12.6 us -> none  [the longest x1 4.51 us: local(): jnp.dot(hidden_units, expert_down[0], preferred_element_type=jnp.float32)]
  transfers between devices with their start and end apart: 5 -> 0, of which waited for: 4 -> 0; matrix products, arithmetic and copies ran while one was open for 8% -> 0% of each run, Pallas kernels for 0% -> 0%
where the time goes in v1:
time: 82 us; the launch traced here: 81 us
  Pallas kernels  55.4 us (68%)
  matrix products  11.4 us (14%)
  other arithmetic  7.04 us (9%)
  local copies, waits for them, and re-layouts  6.47 us (8%)
    pallas_call x1, Pallas kernels, rest(): pl.pallas_call(rest_kernel, out_shape=jax.ShapeDtypeStruct((32, CH), BF),...  55.4 us
    unnamed x21, local copies, waits for them, and re-layouts  4.46 us
    add x1, other arithmetic, local(): keep[:, :, None, None] * state_matrix  4.36 us
    dot_general x1, matrix products, local(): numer = jnp.einsum('shd,shdv->shv', query, new_matrix)  2.95 us

profile of v1, /device:TPU:0, one launch (start us, length us, event | category | flops | bytes accessed | tf_op | source)
XLA Modules:
  0.0 81.0 jit_solution(10844259443844033583)
XLA Ops:
  0.6 0.0 copy-start
  0.7 0.9 %slice.3 = f32[1,2048]{1,0:T(1,128)S(1)} slice(f32[4,2048]{1,0:T(4,128)} %gains.1), slice={[0:1], [0:2048]} | slice | bytes 16384 | tf_op jit(solution)/shard_map/slice | solution.py:395
  1.5 1.0 %fusion.1 = f32[32]{0:T(128)S(1)} fusion(bf16[32,2048]{1,0:T(8,128)(2,1)} %hidden.1), kind=kLoop, calls=%fused_computation.10 | loop fusion | flops 196576 | bytes 131200 | tf_op jit(solution)/shard_map/reduce_sum | solution.py:394
  2.5 1.1 %fusion.8 = f32[32,2]{0,1:T(2,128)S(1)} fusion(bf16[2048,8]{0,1:T(8,128)(2,1)} %param.28, s32[]{:T(128)S(6)} %select_n.10, bf16[32,2048]{1,0:T(8,128)(2,1)} %hidden.1, f32[2048]{0:T(1024)S(1)} %bitcast.23, f32[32]{0:T(128)S(1)} %add_rsqrt_fusion), kind=kOutput, calls=%fused_computation.21 | convolution fusion | flops 524288 | bytes 147844 | tf_op jit(solution)/shard_map/dot_general | solution.py:405
  3.7 0.7 dynamic_slice.10
  4.4 1.2 %subtract_exponential_fusion = (f32[32,2]{0,1:T(2,128)S(1)}, f32[32,2]{0,1:T(2,128)S(1)}) fusion(f32[32,2]{0,1:T(2,128)S(1)} %fusion.8, f32[32,2]{0,1:T(2,128)} %param.34, f32[2]{0:T(128)S(1)} %dynamic_slice.10, bf16[2048,8]{0,1:T(8,128)(2,1)} %param.29, s32[]{:T(128)S(6)} %select_n.10, bf16[32,2048]{1,0:T(8,128)(2,1)} %hidden.1, f32[2048]{0:T(1024)S(1)} %bitcast.24, ...), kind=kOutput, calls=%fused_computation.29 | convolution fusion | flops 525056 | bytes 149388 | tf_op jit(solution)/shard_map/dot_general | solution.py:407
  5.6 0.0 copy-start.5
  5.6 0.1 copy.27
  5.7 0.1 copy.26
  5.8 1.6 %convolution_convert_fusion.3 = bf16[32,256]{1,0:T(8,128)(2,1)S(1)} fusion(bf16[2048,256]{1,0:T(8,128)(2,1)} %param.24, bf16[32,2048]{1,0:T(8,128)(2,1)} %hidden.1, f32[2048]{0:T(1024)S(1)} %bitcast.25, f32[32]{0:T(128)S(1)} %add_rsqrt_fusion), kind=kOutput, calls=%fused_computation.4 | convolution fusion | flops 33824768 | bytes 1204352 | tf_op jit(solution)/shard_map/dot_general | solution.py:397
  7.4 1.6 %convolution_convert_fusion.2 = bf16[32,256]{1,0:T(8,128)(2,1)S(1)} fusion(bf16[2048,256]{1,0:T(8,128)(2,1)} %param.25, bf16[32,2048]{1,0:T(8,128)(2,1)} %hidden.1, f32[2048]{0:T(1024)S(1)} %bitcast.26, f32[32]{0:T(128)S(1)} %add_rsqrt_fusion), kind=kOutput, calls=%fused_computation.3 | convolution fusion | flops 33824768 | bytes 1204352 | tf_op jit(solution)/shard_map/dot_general | solution.py:398
  9.1 1.5 %fusion.5 = (f32[32,2]{1,0:T(8,128)S(1)}, f32[32,2,128]{2,1,0:T(2,128)}, f32[32,2,128]{2,1,0:T(2,128)S(1)}) fusion(bf16[32,2,128]{2,1,0:T(2,128)(2,1)S(1)} %reshape.48, f32[32,2,128]{2,1,0:T(2,128)} %param.33, f32[32,2]{1,0:T(8,128)S(1)} %copy.26, f32[32,2,128]{2,1,0:T(2,128)S(1)} %reshape.56, f32[32,2]{1,0:T(8,128)S(1)} %copy.27), kind=kLoop, calls=%fused_computation.16 | loop fusion | flops 49088 | bytes 148224
  10.6 1.6 %convolution_convert_fusion.1 = bf16[32,256]{1,0:T(8,128)(2,1)S(1)} fusion(bf16[2048,256]{1,0:T(8,128)(2,1)} %param.26, bf16[32,2048]{1,0:T(8,128)(2,1)} %hidden.1, f32[2048]{0:T(1024)S(1)} %bitcast.27, f32[32]{0:T(128)S(1)} %add_rsqrt_fusion), kind=kOutput, calls=%fused_computation.2 | convolution fusion | flops 33824768 | bytes 1204352 | tf_op jit(solution)/shard_map/dot_general | solution.py:399
  12.3 4.4 %multiply_add_fusion = f32[32,2,128,128]{3,2,1,0:T(8,128)} fusion(f32[32,2,128,128]{3,2,1,0:T(8,128)} %param.32, f32[32,2,128]{2,1,0:T(2,128)S(1)} %reshape.57, f32[32,2,128]{2,1,0:T(2,128)S(1)} %get-tuple-element.6, f32[32,2]{1,0:T(8,128)S(1)} %copy.26), kind=kLoop, calls=%fused_computation | loop fusion | flops 3145728 | bytes 8454400 | tf_op jit(solution)/shard_map/add | solution.py:418
  16.6 0.0 copy-start.1
  16.6 0.0 copy-start.2
  16.6 0.0 copy-start.3
  16.6 0.0 copy-start.4
  16.6 0.0 copy-start.6
  16.7 0.0 copy-start.7
  16.7 3.0 %fusion.24 = f32[32,2,1,128]{3,2,1,0:T(1,128)S(1)} fusion(bf16[32,2,128,1]{2,3,1,0:T(2,128)(2,1)S(1)} %reshape.63, f32[32,2,128,128]{3,2,1,0:T(8,128)} %multiply_add_fusion), kind=kOutput, calls=%fused_computation.34 | convolution fusion | flops 2097152 | bytes 4243456 | tf_op jit(solution)/shard_map/shd,shdv->shv/dot_general | solution.py:421
  19.6 0.1 copy.39
  19.7 0.0 copy-done.5
  19.7 0.1 copy.29
  19.8 0.1 broadcast_divide_fusion
  19.9 0.0 copy-done.1
  19.9 0.0 copy-done.2
  20.0 0.3 convolution_convert_fusion.4
  20.3 0.0 copy-done
  20.3 0.9 %convolution_convert_fusion.terms = bf16[32,2048]{1,0:T(8,128)(2,1)} fusion(bf16[256,2048]{1,0:T(8,128)(2,1)S(1)} %copy-done, f32[4,8,2,128]{3,2,1,0:T(2,128)S(1)} %bitcast.30, bf16[32,256]{1,0:T(8,128)(2,1)S(1)} %convolution_convert_fusion.4), kind=kOutput, calls=%fused_computation.1 | convolution fusion | flops 33669120 | bytes 1228800 | tf_op jit(solution)/shard_map/dot_general | solution.py:427
  21.2 0.0 copy-done.3
  21.2 0.8 %copy.32.dg = bf16[512,176]{1,0:T(8,128)(2,1)} copy(bf16[512,176]{0,1:T(8,128)(2,1)S(1)} %copy-done.3) | data formatting | bytes 360448 | tf_op args[18]
  22.1 0.0 copy-done.4
  22.1 0.8 %copy.33.du = bf16[512,176]{1,0:T(8,128)(2,1)} copy(bf16[512,176]{0,1:T(8,128)(2,1)S(1)} %copy-done.4) | data formatting | bytes 360448 | tf_op args[19]
  22.9 0.0 copy-done.6
  22.9 0.7 copy.30.routes
  23.6 0.0 copy-done.7
  23.6 0.7 copy.31.scores
  24.3 55.4 %rest.1 = bf16[32,512]{1,0:T(8,128)(2,1)} custom-call(bf16[32,2048]{1,0:T(8,128)(2,1)} %convolution_convert_fusion.terms, bf16[32,2048]{1,0:T(8,128)(2,1)} %hidden.1, f32[4,2048]{1,0:T(4,128)} %gains.1, f32[1,2048]{1,0:T(1,128)} %bitcast.31, s32[32,2]{1,0:T(8,128)} %copy.30.routes, f32[32,2]{1,0:T(8,128)} %copy.31.scores, bf16[4,512,896]{2,1,0:T(8,128)(2,1)} %bitcast.20, ...), custom_call_target="tpu_custom_call" | custom-call | tf_op jit(solution)/shard_map/rest/pallas_call | solution.py:332
  79.6 1.4 %copy.45 = bf16[32,512]{1,0:T(8,128)(2,1)} copy(bf16[32,512]{1,0:T(8,128)(2,1)} %rest.1) | data formatting | bytes 65536
  (7 shorter events, 0.1 us)
Async XLA Ops:
  0.6 19.7 %copy-start = (bf16[256,2048]{1,0:T(8,128)(2,1)S(1)}, bf16[256,2048]{1,0:T(8,128)(2,1)}, u32[]{:S(2)}) copy-start(bf16[256,2048]{1,0:T(8,128)(2,1)} %param.31) | copy-start | bytes 3145732
  5.6 14.1 %copy-start.5 = (f32[32,2]{0,1:T(2,128)}, f32[32,2]{0,1:T(2,128)S(1)}, u32[]{:S(2)}) copy-start(f32[32,2]{0,1:T(2,128)S(1)} %get-tuple-element.16) | copy-start | bytes 772
  16.6 3.3 %copy-start.1 = (bf16[32,2048]{1,0:T(8,128)(2,1)S(1)}, bf16[32,2048]{1,0:T(8,128)(2,1)}, u32[]{:S(2)}) copy-start(bf16[32,2048]{1,0:T(8,128)(2,1)} %hidden.1) | copy-start | bytes 393220
  16.6 3.3 %copy-start.2 = (bf16[2048,256]{1,0:T(8,128)(2,1)S(1)}, bf16[2048,256]{1,0:T(8,128)(2,1)}, u32[]{:S(2)}) copy-start(bf16[2048,256]{1,0:T(8,128)(2,1)} %param.27) | copy-start | bytes 3145732
  16.6 4.6 %copy-start.3 = (bf16[512,176]{0,1:T(8,128)(2,1)S(1)}, bf16[512,176]{0,1:T(8,128)(2,1)}, u32[]{:S(2)}) copy-start(bf16[512,176]{0,1:T(8,128)(2,1)} %param.40) | copy-start | bytes 540676
  16.6 5.4 %copy-start.4 = (bf16[512,176]{0,1:T(8,128)(2,1)S(1)}, bf16[512,176]{0,1:T(8,128)(2,1)}, u32[]{:S(2)}) copy-start(bf16[512,176]{0,1:T(8,128)(2,1)} %param.41) | copy-start | bytes 540676
  16.6 6.3 %copy-start.6 = (s32[32,2]{0,1:T(2,128)S(1)}, s32[32,2]{0,1:T(2,128)}, u32[]{:S(2)}) copy-start(s32[32,2]{0,1:T(2,128)} %param.35) | copy-start | bytes 772
  16.7 6.9 %copy-start.7 = (f32[32,2]{0,1:T(2,128)S(1)}, f32[32,2]{0,1:T(2,128)}, u32[]{:S(2)}) copy-start(f32[32,2]{0,1:T(2,128)} %param.36) | copy-start | bytes 772

commit v2 on v1

v2 whole, which is shorter than its diff:
```python
import jax
import jax.numpy as jnp
from jax import lax
from jax.experimental import pallas as pl
from jax.experimental.pallas import tpu as pltpu
from jax.sharding import PartitionSpec as P

EPS = 1e-06
MESH = pl.DeviceIdType.MESH
BF = jnp.bfloat16
F32 = jnp.float32
I32 = jnp.int32
CH = 512


def dot(a, b):
    return jnp.dot(a, b, preferred_element_type=F32)


def iota(shape, dim):
    return lax.broadcasted_iota(I32, shape, dim)


def one_hot(columns, rows, target):
    return (iota((rows, columns), 1) == target(iota((rows, columns), 0))).astype(BF)


def stacked(ref):
    return jnp.concatenate([ref[:, q * CH : (q + 1) * CH] for q in range(4)], axis=0)


def row_total(values):
    part = jnp.sum(values, axis=1, keepdims=True)
    total = part[0:8] + part[8:16] + part[16:24] + part[24:32]
    return jnp.concatenate([total] * 4, axis=0)


def silu(t):
    return t / (1.0 + jnp.exp(-t))


def whole_kernel(
    hidden, gains, mix, routes, scores, w_in, w_fg, bias, smax, snorm,
    wq_h, wk_h, wv_h, wo_h, wm_h, st_h, eg, eu, ed, dg, du, dd,
    out, keep_out, written_out, value_out, norm_out, max_out,
    wq, wk, wv, wo, wm, st, numer,
    wg, wu, wd, gbuf, ubuf, dbuf,
    bsend, brecv, hperm, nall, tok, osend, orecv, rsend, rrecv, dsend, drecv,
    msend, mrecv, fsend, frecv,
    pm, pmi, pd, pdi, gk, xs, xd, ys, yd, hexp, hden, resid_s, mixg_s, share_s,
    load_sem, b_sem, n_sem, t_sem, o_sem, r_sem, d_sem, m_sem, f_sem,
    gs_sem, gr_sem, us_sem, ur_sem, ds_sem, dr_sem,
):
    x = lax.axis_index("tp")
    ep = lax.axis_index("ep")
    c = ep % 2
    y = (ep // 2) % 4
    z = ep // 8
    p = ep // 2
    mate = p * 2 + (1 - c)
    left, right, far = (x + 3) % 4, (x + 1) % 4, (x + 2) % 4

    def plane(k):
        return ((z + k // 8) % 4) * 8 + ((y + (k // 2) % 4) % 4) * 2 + (c + k % 2) % 2

    def remote(src, dst, ssem, rsem, to_ep, to_x):
        return pltpu.make_async_remote_copy(
            src_ref=src, dst_ref=dst, send_sem=ssem, recv_sem=rsem,
            device_id=(to_ep, to_x), device_id_type=MESH,
        )

    def landed(ref, sem):
        pltpu.make_async_copy(ref, ref, sem).wait()

    barrier = pltpu.get_barrier_semaphore()

    def greet(k, carry):
        pl.semaphore_signal(barrier, inc=1, device_id=(plane(k), x), device_id_type=MESH)
        return carry

    loads = [
        pltpu.make_async_copy(src, dst, load_sem.at[n])
        for n, (src, dst) in enumerate(
            [
                (wq_h, wq), (wk_h, wk), (wv_h, wv), (wo_h, wo),
                (dg, gbuf.at[c, x]), (du, ubuf.at[c, x]), (dd, dbuf.at[c, x]),
                (st_h, st), (wm_h, wm), (eg, wg), (eu, wu), (ed, wd),
            ]
        )
    ]
    for load in loads:
        load.start()
    for d in (2, 1, 3):
        pl.semaphore_signal(barrier, inc=1, device_id=(ep, (x + d) % 4), device_id_type=MESH)
    lax.fori_loop(1, 32, greet, 0)

    def first_round(buf, ssem, rsem):
        block = buf.at[c, x]
        copies = [
            remote(block, block, ssem.at[0], rsem.at[0], ep, right),
            remote(block, block, ssem.at[1], rsem.at[1], ep, left),
            remote(block, block, ssem.at[4], rsem.at[4], mate, x),
        ]
        for copy in copies:
            copy.start()
        return copies

    def second_round(buf, ssem, rsem):
        from_left, from_right = buf.at[c, left], buf.at[c, right]
        low = buf.at[c, left, pl.ds(0, 96)]
        high = buf.at[c, right, pl.ds(96, 80)]
        copies = [
            remote(low, low, ssem.at[2], rsem.at[2], ep, right),
            remote(from_left, from_left, ssem.at[5], rsem.at[5], mate, x),
            remote(high, high, ssem.at[3], rsem.at[3], ep, left),
            remote(from_right, from_right, ssem.at[6], rsem.at[6], mate, x),
        ]
        landed(from_left, rsem.at[0])
        copies[0].start()
        copies[1].start()
        landed(from_right, rsem.at[1])
        copies[2].start()
        copies[3].start()
        return copies

    def third_round(buf, ssem, rsem):
        block = buf.at[c, far]
        landed(buf.at[c, far, pl.ds(0, 96)], rsem.at[2])
        landed(buf.at[c, far, pl.ds(96, 80)], rsem.at[3])
        copy = remote(block, block, ssem.at[7], rsem.at[7], mate, x)
        copy.start()
        return [copy]

    def from_mate(buf, rsem):
        for n, place in ((4, x), (5, left), (6, right), (7, far)):
            landed(buf.at[1 - c, place], rsem.at[n])

    start_f = hidden[...].astype(F32)
    start_scale = lax.rsqrt(jnp.sum(start_f * start_f, axis=1, keepdims=True) / 2048.0 + EPS)
    normed_in = (start_f * start_scale * gains[0:1, :]).astype(BF)
    same = iota((32, 32), 0) == iota((32, 32), 1)

    def as_column(row):
        return jnp.sum(jnp.where(same, jnp.broadcast_to(row, (32, 32)), 0.0), axis=1, keepdims=True)

    def as_row(column):
        return jnp.sum(jnp.where(same, jnp.broadcast_to(column, (32, 32)), 0.0), axis=0, keepdims=True)

    def along(a, b):
        return lax.dot_general(a, b, (((1,), (1,)), ((), ())), preferred_element_type=F32)

    gate_in = along(normed_in, w_in[...])
    forget = along(normed_in, w_fg[...]) + bias[...]
    forget = jnp.minimum(forget, 0.0) - jnp.log(1.0 + jnp.exp(-jnp.abs(forget)))
    head8 = iota((32, 8), 1)
    keeps, writes, floors = [], [], []
    for h in range(2):
        mine = head8 == 2 * x + h
        in_gate = jnp.sum(jnp.where(mine, gate_in, 0.0), axis=1, keepdims=True)
        carried = jnp.sum(jnp.where(mine, forget, 0.0), axis=1, keepdims=True) + as_column(smax[h : h + 1, :])
        new_max = jnp.maximum(carried, in_gate)
        keeps.append(jnp.exp(carried - new_max))
        writes.append(jnp.exp(in_gate - new_max))
        floors.append(jnp.exp(-new_max))
        max_out[h : h + 1, :] = as_row(new_max)
    loads[0].wait()
    query = dot(normed_in, wq[...]).astype(BF)
    loads[1].wait()
    keys = dot(normed_in, wk[...]).astype(BF).astype(F32) * 128.0 ** (-0.5)
    loads[2].wait()
    value = dot(normed_in, wv[...]).astype(BF).astype(F32)
    loads[3].wait()
    out_gate = dot(normed_in, wo[...]).astype(BF).astype(F32)

    pl.semaphore_wait(barrier, 34)
    loads[4].wait()
    weight_out = first_round(gbuf, gs_sem, gr_sem)

    eye = same.astype(BF)
    loads[7].wait()
    mixed = []
    for h in range(2):
        lanes = slice(h * 128, (h + 1) * 128)
        query_t = lax.dot_general(
            query[:, lanes], eye, (((0,), (0,)), ((), ())), preferred_element_type=F32
        )
        for s in range(32):
            numer[h, s : s + 1, :] = jnp.sum(
                query_t[:, s : s + 1] * st[s * 2 + h], axis=0, keepdims=True
            )
        q = query[:, lanes].astype(F32)
        written = writes[h] * keys[:, lanes]
        new_norm = keeps[h] * snorm[:, h, :] + written
        top = keeps[h] * numer[h] + jnp.sum(q * written, axis=1, keepdims=True) * value[:, lanes]
        denom = jnp.sum(q * new_norm, axis=1, keepdims=True)
        read = top / jnp.maximum(jnp.abs(denom), floors[h])
        mixed.append((read / (1.0 + jnp.exp(-out_gate[:, lanes]))).astype(BF))
        keep_out[h] = jnp.broadcast_to(keeps[h], (32, 128))
        written_out[h] = written
        value_out[h] = value[:, lanes]
        norm_out[h] = new_norm
    loads[8].wait()
    share = [
        (dot(mixed[0], wm[0:128, q * CH : (q + 1) * CH]) + dot(mixed[1], wm[128:256, q * CH : (q + 1) * CH])).astype(BF)
        for q in range(4)
    ]

    order = one_hot(128, 128, lambda r: ((r >> 3) & 3) * 32 + (r >> 5) * 8 + (r & 7))
    bsend[...] = dot(order, jnp.concatenate(share, axis=0)).astype(BF).reshape(4, 32, CH)
    brecv[x] = bsend[x]
    branch_out = []
    for d in (2, 1, 3):
        to = (x + d) % 4
        branch_out.append(remote(bsend.at[to], brecv.at[x], b_sem.at[0], b_sem.at[1], ep, to))
        branch_out[-1].start()

    loads[5].wait()
    weight_out += first_round(ubuf, us_sem, ur_sem)
    hperm[...] = dot(order, stacked(hidden)).reshape(4, 32, CH)

    expert0, expert1 = as_column(routes[0:1, :].astype(F32)), as_column(routes[1:2, :].astype(F32))
    lane32 = iota((32, 32), 1)
    lane32_f = lane32.astype(F32)
    hot0 = (lane32_f == expert0).astype(F32)
    hot1 = (lane32_f == expert1).astype(F32)
    earlier = (iota((32, 32), 0) > lane32).astype(BF)
    before = dot(earlier, (hot0 + hot1).astype(BF))
    score0, score1 = as_column(scores[0:1, :]), as_column(scores[1:2, :])
    whole = score0 + score1

    def by_piece(column, step):
        return jnp.concatenate(
            [column[xx * 8 : xx * 8 + 8] + q * step for xx in range(4) for q in range(4)], axis=0
        )

    for k, (expert, hot, score) in enumerate(((expert0, hot0, score0), (expert1, hot1, score1))):
        rank = jnp.sum(hot * before, axis=1, keepdims=True)
        place = by_piece((expert * 16.0 + rank).astype(I32), 4)
        gk[k] = (iota((128, 512), 1) == place).astype(BF)
        share_s[k] = jnp.broadcast_to(by_piece(score / whole, 0.0), (128, 128))
    pm[...] = one_hot(512, 512, lambda r: ((r >> 2) & 31) * 16 + (r >> 7) * 4 + (r & 3))
    pmi[...] = one_hot(512, 512, lambda r: ((r >> 2) & 3) * 128 + (r >> 4) * 4 + (r & 3))
    pd[...] = one_hot(512, 512, lambda r: ((r >> 3) & 15) * 32 + (r >> 7) * 8 + (r & 7))
    pdi[...] = one_hot(512, 512, lambda r: ((r >> 3) & 3) * 128 + (r >> 5) * 8 + (r & 7))

    def gain(k):
        return jnp.concatenate(
            [jnp.broadcast_to(gains[k : k + 1, q * CH : (q + 1) * CH], (8, CH)) for q in range(4)],
            axis=0,
        )

    mix_rows = jnp.concatenate(
        [jnp.broadcast_to(mix[0:1, q * CH : (q + 1) * CH], (8, CH)) for q in range(4)], axis=0
    )

    landed(brecv.at[pl.ds(0, 3)], b_sem.at[1])
    branch = brecv[0].astype(F32) + brecv[1].astype(F32) + brecv[2].astype(F32) + brecv[3].astype(F32)
    branch = branch.astype(BF).astype(F32)
    residual_f = hperm[x] + gain(1) * branch * lax.rsqrt(row_total(branch * branch) / 2048.0 + EPS)
    scale_two = lax.rsqrt(row_total(residual_f * residual_f) / 2048.0 + EPS)
    normed = (residual_f * scale_two * gain(2)).astype(BF)
    nall[x] = normed
    tok[p] = normed

    token_out = []
    for d in (2, 1, 3):
        to = (x + d) % 4
        token_out.append(remote(nall.at[x], nall.at[x], n_sem.at[0], n_sem.at[1], ep, to))
        token_out[-1].start()

    def share_tokens(k, carry):
        to = ((z + k // 4) % 4) * 8 + ((y + k % 4) % 4) * 2 + c
        remote(nall.at[x], tok.at[p], t_sem.at[0], t_sem.at[1], to, x).start()
        return carry

    lax.fori_loop(1, 16, share_tokens, 0)
    weight_out += second_round(gbuf, gs_sem, gr_sem)
    resid_s[...] = residual_f.astype(BF).astype(F32)
    mix_dot = scale_two * row_total(residual_f * gain(2) * mix_rows)
    mixg_s[...] = jnp.broadcast_to(1.0 / (1.0 + jnp.exp(-mix_dot)), (32, 128))

    landed(nall.at[pl.ds(0, 3)], n_sem.at[1])
    chosen = gk[0] + gk[1]
    rows = lax.dot_general(
        chosen, nall[...].reshape(128, CH), (((0,), (0,)), ((), ())), preferred_element_type=F32
    )
    osend[...] = rows.astype(BF).reshape(32, 16, CH)
    orecv[ep] = osend[ep]

    def dispatch(k, carry):
        to = plane(k)
        remote(osend.at[to], orecv.at[ep], o_sem.at[0], o_sem.at[1], to, x).start()
        return carry

    lax.fori_loop(1, 32, dispatch, 0)

    loads[6].wait()
    weight_out += second_round(ubuf, us_sem, ur_sem)
    weight_out += first_round(dbuf, ds_sem, dr_sem)
    weight_out += third_round(gbuf, gs_sem, gr_sem)
    weight_out += third_round(ubuf, us_sem, ur_sem)
    weight_out += second_round(dbuf, ds_sem, dr_sem)

    landed(tok.at[pl.ds(0, 15)], t_sem.at[1])
    xd[...] = dot(pd[...], tok[...].reshape(512, CH)).astype(BF).reshape(4, 128, CH)
    from_mate(gbuf, gr_sem)
    from_mate(ubuf, ur_sem)
    for core in range(2):
        pre_gate = along(xd[0], gbuf[core, 0])
        pre_up = along(xd[0], ubuf[core, 0])
        for q in range(1, 4):
            pre_gate += along(xd[q], gbuf[core, q])
            pre_up += along(xd[q], ubuf[core, q])
        hden[core] = (silu(pre_gate) * pre_up).astype(BF)
    weight_out += third_round(dbuf, ds_sem, dr_sem)
    from_mate(dbuf, dr_sem)
    for q in range(4):
        yd[q * 128 : (q + 1) * 128] = (
            dot(hden[0], dbuf[0, q]) + dot(hden[1], dbuf[1, q])
        ).astype(BF)
    dsend[...] = dot(pdi[...], yd[...]).astype(BF).reshape(16, 32, CH)
    drecv[p] = dsend[p]

    def dense_back(k, carry):
        to = ((z + k // 4) % 4) * 4 + (y + k % 4) % 4
        remote(dsend.at[to], drecv.at[p], d_sem.at[0], d_sem.at[1], to * 2 + c, x).start()
        return carry

    lax.fori_loop(1, 16, dense_back, 0)

    landed(orecv.at[pl.ds(0, 31)], o_sem.at[1])
    xs[...] = dot(pm[...], orecv[...].reshape(512, CH)).astype(BF).reshape(4, 128, CH)
    loads[9].wait()
    loads[10].wait()
    gate_pre = dot(xs[0], wg[0])
    up_pre = dot(xs[0], wu[0])
    for q in range(1, 4):
        gate_pre += dot(xs[q], wg[q])
        up_pre += dot(xs[q], wu[q])
    hexp[...] = (silu(gate_pre) * up_pre).astype(BF)
    loads[11].wait()
    for q in range(4):
        ys[q * 128 : (q + 1) * 128] = dot(hexp[...], wd[:, q * CH : (q + 1) * CH]).astype(BF)
    rsend[...] = dot(pmi[...], ys[...]).astype(BF).reshape(32, 16, CH)
    rrecv[ep] = rsend[ep]

    def give_back(k, carry):
        to = plane(k)
        remote(rsend.at[to], rrecv.at[ep], r_sem.at[0], r_sem.at[1], to, x).start()
        return carry

    lax.fori_loop(1, 32, give_back, 0)

    landed(rrecv.at[pl.ds(0, 31)], r_sem.at[1])
    back = rrecv[...].reshape(512, CH)
    moe = share_s[0][:, 0:1] * dot(gk[0], back) + share_s[1][:, 0:1] * dot(gk[1], back)
    msend[...] = moe.astype(BF).reshape(4, 32, CH)
    mrecv[x] = msend[x]
    moe_out = []
    for d in (2, 1, 3):
        to = (x + d) % 4
        moe_out.append(remote(msend.at[to], mrecv.at[x], m_sem.at[0], m_sem.at[1], ep, to))
        moe_out[-1].start()

    landed(drecv.at[pl.ds(0, 15)], d_sem.at[1])
    dense = drecv[0].astype(F32)
    for n in range(1, 16):
        dense += drecv[n].astype(F32)
    landed(mrecv.at[pl.ds(0, 3)], m_sem.at[1])
    ffn = mrecv[0].astype(F32) + mrecv[1].astype(F32) + mrecv[2].astype(F32) + mrecv[3].astype(F32)
    ffn += mixg_s[:, 0:1] * dense
    scale_ffn = lax.rsqrt(row_total(ffn * ffn) / 2048.0 + EPS)
    fsend[...] = (resid_s[...] + gain(3) * ffn * scale_ffn).reshape(4, 8, CH)
    frecv[x] = fsend[x]
    last_out = []
    for d in (2, 1, 3):
        to = (x + d) % 4
        last_out.append(remote(fsend.at[to], frecv.at[x], f_sem.at[0], f_sem.at[1], ep, to))
        last_out[-1].start()

    for copy in weight_out:
        copy.wait_send()
    landed(bsend.at[pl.ds(0, 3)], b_sem.at[0])
    landed(nall.at[pl.ds(0, 3)], n_sem.at[0])
    landed(tok.at[pl.ds(0, 15)], t_sem.at[0])
    landed(osend.at[pl.ds(0, 31)], o_sem.at[0])
    landed(rsend.at[pl.ds(0, 31)], r_sem.at[0])
    landed(dsend.at[pl.ds(0, 15)], d_sem.at[0])
    landed(msend.at[pl.ds(0, 3)], m_sem.at[0])
    landed(frecv.at[pl.ds(0, 3)], f_sem.at[1])
    out[...] = frecv[...].reshape(32, CH).astype(BF)
    landed(fsend.at[pl.ds(0, 3)], f_sem.at[0])


def whole(small, large):
    V = pltpu.VMEM
    dma = pltpu.SemaphoreType.DMA
    vm = pl.BlockSpec(memory_space=pltpu.VMEM)
    hb = pl.BlockSpec(memory_space=pl.ANY)
    head = jax.ShapeDtypeStruct((2, 32, 128), F32)
    return pl.pallas_call(
        whole_kernel,
        out_shape=(
            jax.ShapeDtypeStruct((32, CH), BF), head, head, head, head,
            jax.ShapeDtypeStruct((2, 32), F32),
        ),
        in_specs=[vm] * len(small) + [hb] * len(large),
        out_specs=(vm,) * 6,
        scratch_shapes=[
            V((2048, 256), BF), V((2048, 256), BF), V((2048, 256), BF), V((2048, 256), BF),
            V((256, 2048), BF), V((64, 128, 128), F32), V((2, 32, 128), F32),
            V((4, 512, 896), BF), V((4, 512, 896), BF), V((896, 2048), BF),
            V((2, 4, 176, 512), BF), V((2, 4, 176, 512), BF), V((2, 4, 176, 512), BF),
            V((4, 32, CH), BF), V((4, 32, CH), BF), V((4, 32, CH), F32), V((4, 32, CH), BF),
            V((16, 32, CH), BF),
            V((32, 16, CH), BF), V((32, 16, CH), BF), V((32, 16, CH), BF), V((32, 16, CH), BF),
            V((16, 32, CH), BF), V((16, 32, CH), BF),
            V((4, 32, CH), BF), V((4, 32, CH), BF), V((4, 8, CH), F32), V((4, 8, CH), F32),
            V((512, 512), BF), V((512, 512), BF), V((512, 512), BF), V((512, 512), BF),
            V((2, 128, 512), BF), V((4, 128, CH), BF), V((4, 128, CH), BF),
            V((512, CH), BF), V((512, CH), BF), V((128, 896), BF), V((2, 128, 176), BF),
            V((32, CH), F32), V((32, 128), F32), V((2, 128, 128), F32),
            dma((12,)), dma((2,)), dma((2,)), dma((2,)), dma((2,)), dma((2,)), dma((2,)),
            dma((2,)), dma((2,)), dma((8,)), dma((8,)), dma((8,)), dma((8,)), dma((8,)), dma((8,)),
        ],
        compiler_params=pltpu.CompilerParams(
            collective_id=0, has_side_effects=True, vmem_limit_bytes=60 * 1024 * 1024
        ),
        name="whole",
    )(*small, *large)


def memory_kernel(
    state, keep, written, value, norm, top, hidden_in, matrix_out, norm_out, top_out, hidden_out
):
    spot = iota((8, 128), 0)
    for h in range(2):
        w = written[h]
        high = w.astype(BF).astype(F32)
        low = w - high
        both = jnp.concatenate([value[h], value[h]], axis=0).astype(BF)
        norm_out[:, h, :] = norm[h]
        for s in range(8):
            sides = jnp.concatenate(
                [jnp.where(spot == s, high, 0.0), jnp.where(spot == s, low, 0.0)], axis=0
            ).astype(BF)
            outer = lax.dot_general(sides, both, (((0,), (0,)), ((), ())), preferred_element_type=F32)
            matrix_out[s, h] = keep[h, s : s + 1, :] * state[s, h] + outer
    top_out[...] = top[...]
    hidden_out[...] = hidden_in[...]


def memory(state, keep, written, value, norm, top, hidden_in):
    part = pl.BlockSpec((2, 8, 128), lambda n: (0, n, 0))
    fixed2 = pl.BlockSpec((2, 32), lambda n: (0, 0))
    fixed = pl.BlockSpec((32, CH), lambda n: (0, 0))
    block = pl.BlockSpec((8, 2, 128, 128), lambda n: (n, 0, 0, 0))
    return pl.pallas_call(
        memory_kernel,
        grid=(4,),
        out_shape=(
            jax.ShapeDtypeStruct((32, 2, 128, 128), F32),
            jax.ShapeDtypeStruct((32, 2, 128), F32),
            jax.ShapeDtypeStruct((2, 32), F32),
            jax.ShapeDtypeStruct((32, CH), BF),
        ),
        in_specs=[block, part, part, part, part, fixed2, fixed],
        out_specs=(block, pl.BlockSpec((8, 2, 128), lambda n: (n, 0, 0)), fixed2, fixed),
        name="memory",
    )(state, keep, written, value, norm, top, hidden_in)


def local(
    hidden,
    norm_gains,
    w_query,
    w_key,
    w_value,
    w_outgate,
    w_input_gate,
    w_forget_gate,
    forget_bias,
    w_mix_out,
    state_matrix,
    state_norm,
    state_max,
    routes,
    route_scores,
    expert_gate,
    expert_up,
    expert_down,
    dense_gate,
    dense_up,
    dense_down,
    dense_mix,
):
    new_hidden, keep, written, value, norm, top = whole(
        (
            hidden, norm_gains, dense_mix.reshape(1, -1), routes.T, route_scores.T,
            w_input_gate.T, w_forget_gate.T, forget_bias.reshape(1, -1), state_max.T, state_norm,
        ),
        (
            w_query, w_key, w_value, w_outgate, w_mix_out, state_matrix.reshape(64, 128, 128),
            expert_gate.reshape(4, CH, -1), expert_up.reshape(4, CH, -1), expert_down[0],
            dense_gate.T, dense_up.T, dense_down,
        ),
    )
    new_matrix, new_norm, new_top, new_hidden = memory(
        state_matrix, keep, written, value, norm, top, new_hidden
    )
    return (new_hidden, new_matrix, new_norm, new_top.T)


def solution(mesh):
    placed = (
        P("ep", None),
        P(),
        P(None, "tp"),
        P(None, "tp"),
        P(None, "tp"),
        P(None, "tp"),
        P(),
        P(),
        P(),
        P("tp", None),
        P("ep", "tp", None, None),
        P("ep", "tp", None),
        P("ep", "tp"),
        P("ep", None),
        P("ep", None),
        P("ep", None, "tp"),
        P("ep", None, "tp"),
        P("ep", "tp", None),
        P("tp", "ep"),
        P("tp", "ep"),
        P("ep", "tp"),
        P(),
    )
    return jax.shard_map(
        local,
        mesh=mesh,
        in_specs=placed,
        out_specs=(P("ep", "tp"), P("ep", "tp", None, None), P("ep", "tp", None), P("ep", "tp")),
        check_vma=False,
    )
```

time: 82 us -> 66.6 us (0.81)
  matrix products: 11.4 us -> 0 us
  Pallas kernels: 55.4 us -> 65.7 us
  other arithmetic: 7.04 us -> 0 us
  local copies, waits for them, and re-layouts: 6.47 us -> 0 us
    dot_general x8 -> x0, matrix products: 11.4 us -> none  [the longest x1 2.95 us: local(): numer = jnp.einsum('shd,shdv->shv', query, new_matrix)]
    pallas_call x1 -> x2, Pallas kernels: 55.4 us -> 65.7 us  [the longest x1 60.3 us: whole(): pl.pallas_call(whole_kernel, out_shape=(jax.ShapeDtypeStruct((32, CH), BF...]
    unnamed x21 -> x0, local copies, waits for them, and re-layouts: 4.46 us -> none
    add x1 -> x0, other arithmetic: 4.36 us -> none  [local(): keep[:, :, None, None] * state_matrix]
    unnamed x1 -> x0, other arithmetic: 1.51 us -> none
    reduce_sum x1 -> x0, other arithmetic: 1.04 us -> none  [local(): jnp.mean(start_f * start_f, axis=-1, keepdims=True) + EPS]
    slice x1 -> x0, local copies, waits for them, and re-layouts: 0.85 us -> none  [local(): norm_gains[0]]
where the time goes in v2:
time: 66.6 us; the launch traced here: 66.4 us
  Pallas kernels  65.7 us (99%)
    pallas_call x1, Pallas kernels, whole(): pl.pallas_call(whole_kernel, out_shape=(jax.ShapeDtypeStruct((32, CH), BF...  60.3 us
    pallas_call x1, Pallas kernels, memory(): pl.pallas_call(memory_kernel, grid=(4,), out_shape=(jax.ShapeDtypeStruct(...  5.4 us

profile of v2, /device:TPU:0, one launch (start us, length us, event | category | flops | bytes accessed | tf_op | source)
XLA Modules:
  0.0 66.4 jit_solution(2341806273861887909)
XLA Ops:
  0.6 60.3 %whole.1 = (bf16[32,512]{1,0:T(8,128)(2,1)}, f32[2,32,128]{2,1,0:T(8,128)}, f32[2,32,128]{2,1,0:T(8,128)}, f32[2,32,128]{2,1,0:T(8,128)}, f32[2,32,128]{2,1,0:T(8,128)}, /*index=5*/f32[2,32]{1,0:T(2,128)}) custom-call(bf16[32,2048]{1,0:T(8,128)(2,1)} %hidden.1, f32[4,2048]{1,0:T(4,128)} %gains.1, f32[1,2048]{1,0:T(1,128)} %bitcast.22, s32[2,32]{1,0:T(2,128)} %bitcast.23, ...), custom_call_target="tpu_custom_call" | custom-call | tf_op jit(solution)/shard_map/whole/pallas_call | solution.py:401
  61.0 5.4 %memory.1 = (f32[32,2,128,128]{3,2,1,0:T(8,128)}, f32[32,2,128]{2,1,0:T(2,128)}, f32[2,32]{1,0:T(2,128)}, bf16[32,512]{1,0:T(8,128)(2,1)}) custom-call(f32[32,2,128,128]{3,2,1,0:T(8,128)} %state.1, f32[2,32,128]{2,1,0:T(8,128)} %get-tuple-element.14.keep, f32[2,32,128]{2,1,0:T(8,128)} %get-tuple-element.15.written, f32[2,32,128]{2,1,0:T(8,128)} %get-tuple-element.16.value, ...), custom_call_target="tpu_custom_call" | custom-call | tf_op jit(solution)/shard_map/memory/pallas_call | solution.py:458

commit v3 on v2

v3 whole, which is shorter than its diff:
```python
import jax
import jax.numpy as jnp
from jax import lax
from jax.experimental import pallas as pl
from jax.experimental.pallas import tpu as pltpu
from jax.sharding import PartitionSpec as P

EPS = 1e-06
MESH = pl.DeviceIdType.MESH
BF = jnp.bfloat16
F32 = jnp.float32
I32 = jnp.int32
CHIP_STEPS = sorted(
    ((dz, dy) for dz in range(4) for dy in range(4) if dz or dy),
    key=lambda s: -(min(s[0], 4 - s[0]) + min(s[1], 4 - s[1])),
)
PIECES = ((0, 96), (96, 80))
CH = 512


def dot(a, b):
    return jnp.dot(a, b, preferred_element_type=F32)


def iota(shape, dim):
    return lax.broadcasted_iota(I32, shape, dim)


def one_hot(columns, rows, target):
    return (iota((rows, columns), 1) == target(iota((rows, columns), 0))).astype(BF)


def stacked(ref):
    return jnp.concatenate([ref[:, q * CH : (q + 1) * CH] for q in range(4)], axis=0)


def row_total(values):
    part = jnp.sum(values, axis=1, keepdims=True)
    total = part[0:8] + part[8:16] + part[16:24] + part[24:32]
    return jnp.concatenate([total] * 4, axis=0)


def silu(t):
    return t / (1.0 + jnp.exp(-t))


def whole_kernel(
    hidden_h, gains_h, mix_h, routes_h, scores_h, w_in_h, w_fg_h, bias_h, smax_h, snorm_h,
    wq_h, wk_h, wv_h, wo_h, wm_h, st_h, eg, eu, ed, dg, du, dd,
    out, matrix, norm_out, max_out,
    hidden, gains, mix, routes, scores, w_in, w_fg, bias, smax, snorm,
    wq, wk, wv, wo, wm, st, numer,
    wg, wu, wd, gbuf, ubuf, dbuf,
    bsend, brecv, hperm, nall, tok, osend, orecv, rsend, rrecv, dsend, drecv,
    msend, mrecv, fsend, frecv,
    pm, pmi, pd, pdi, gk, xs, xd, ys, yd, hexp, hden, resid_s, mixg_s, share_s,
    load_sem, b_sem, n_sem, t_sem, o_sem, r_sem, d_sem, m_sem, f_sem,
    gs_sem, gr_sem, us_sem, ur_sem, ds_sem, dr_sem,
):
    x = lax.axis_index("tp")
    ep = lax.axis_index("ep")
    c = ep % 2
    y = (ep // 2) % 4
    z = ep // 8
    p = ep // 2
    mate = p * 2 + (1 - c)
    left, right, far = (x + 3) % 4, (x + 1) % 4, (x + 2) % 4

    z_at = [((z + d) % 4) * 8 for d in range(4)]
    y_at = [((y + d) % 4) * 2 for d in range(4)]
    core_at = [c, 1 - c]
    places = [((z + dz) % 4) * 4 + (y + dy) % 4 for dz, dy in CHIP_STEPS]
    chips = [z_at[dz] + y_at[dy] for dz, dy in CHIP_STEPS]
    peers = [base + core for base in chips for core in core_at]
    peers.append(p * 2 + core_at[1])

    def remote(src, dst, ssem, rsem, to_ep, to_x):
        return pltpu.make_async_remote_copy(
            src_ref=src, dst_ref=dst, send_sem=ssem, recv_sem=rsem,
            device_id=(to_ep, to_x), device_id_type=MESH,
        )

    def landed(ref, sem):
        pltpu.make_async_copy(ref, ref, sem).wait()

    barrier = pltpu.get_barrier_semaphore()

    loads = {
        name: pltpu.make_async_copy(src, dst, load_sem.at[n])
        for n, (name, src, dst) in enumerate(
            [
                ("hidden", hidden_h, hidden), ("gains", gains_h, gains),
                ("wq", wq_h, wq), ("wk", wk_h, wk), ("w_in", w_in_h, w_in), ("w_fg", w_fg_h, w_fg),
                ("bias", bias_h, bias), ("smax", smax_h, smax), ("wv", wv_h, wv), ("wo", wo_h, wo),
                ("gate", dg, gbuf.at[c, x]), ("st", st_h, st), ("snorm", snorm_h, snorm), ("wm", wm_h, wm),
                ("up", du, ubuf.at[c, x]), ("down", dd, dbuf.at[c, x]), ("mix", mix_h, mix),
                ("routes", routes_h, routes), ("scores", scores_h, scores),
                ("eg", eg, wg), ("eu", eu, wu), ("ed", ed, wd),
            ]
        )
    }
    for name in ("hidden", "gains", "wq", "wk"):
        loads[name].start()
    for d in (2, 1, 3):
        pl.semaphore_signal(barrier, inc=1, device_id=(ep, (x + d) % 4), device_id_type=MESH)
    for peer in peers:
        pl.semaphore_signal(barrier, inc=1, device_id=(peer, x), device_id_type=MESH)
    for name, load in loads.items():
        if name not in ("hidden", "gains", "wq", "wk"):
            load.start()

    def first_round(weight, part):
        buf, ssem, rsem = weight
        copies = []
        for piece, to in ((0, right), (1, left)) if part == 0 else ((1, right), (0, left)):
            block = buf.at[c, x, pl.ds(*PIECES[piece])]
            n = 2 * part + piece
            copies.append(remote(block, block, ssem.at[n], rsem.at[n], ep, to))
        if part == 1:
            block = buf.at[c, x]
            copies.append(remote(block, block, ssem.at[6], rsem.at[6], mate, x))
        for copy in copies:
            copy.start()
        return copies

    def second_round(weight):
        buf, ssem, rsem = weight
        copies = []
        for piece, near, onward in ((0, left, right), (1, right, left)):
            block = buf.at[c, near, pl.ds(*PIECES[piece])]
            landed(block, rsem.at[piece])
            copies.append(remote(block, block, ssem.at[4 + piece], rsem.at[4 + piece], ep, onward))
            copies[-1].start()
        return copies

    def near_to_mate(weight):
        buf, ssem, rsem = weight
        copies = []
        for piece, n, near in ((1, 7, left), (0, 8, right)):
            landed(buf.at[c, near, pl.ds(*PIECES[piece])], rsem.at[2 + piece])
            block = buf.at[c, near]
            copies.append(remote(block, block, ssem.at[n], rsem.at[n], mate, x))
            copies[-1].start()
        return copies

    def far_to_mate(weight):
        buf, ssem, rsem = weight
        copies = []
        for piece in range(2):
            block = buf.at[c, far, pl.ds(*PIECES[piece])]
            landed(block, rsem.at[4 + piece])
            copies.append(remote(block, block, ssem.at[9 + piece], rsem.at[9 + piece], mate, x))
            copies[-1].start()
        return copies

    def from_mate(weight):
        buf, _, rsem = weight
        for n, place in ((6, x), (7, left), (8, right)):
            landed(buf.at[1 - c, place], rsem.at[n])
        for piece in range(2):
            landed(buf.at[1 - c, far, pl.ds(*PIECES[piece])], rsem.at[9 + piece])

    gate_w = (gbuf, gs_sem, gr_sem)
    up_w = (ubuf, us_sem, ur_sem)
    down_w = (dbuf, ds_sem, dr_sem)

    loads["hidden"].wait()
    start_f = hidden[...].astype(F32)
    start_scale = lax.rsqrt(jnp.sum(start_f * start_f, axis=1, keepdims=True) / 2048.0 + EPS)
    loads["gains"].wait()
    normed_in = (start_f * start_scale * gains[0:1, :]).astype(BF)
    same = iota((32, 32), 0) == iota((32, 32), 1)

    def as_column(row):
        return jnp.sum(jnp.where(same, jnp.broadcast_to(row, (32, 32)), 0.0), axis=1, keepdims=True)

    def as_row(column):
        return jnp.sum(jnp.where(same, jnp.broadcast_to(column, (32, 32)), 0.0), axis=0, keepdims=True)

    def along(a, b):
        return lax.dot_general(a, b, (((1,), (1,)), ((), ())), preferred_element_type=F32)

    loads["wq"].wait()
    query = dot(normed_in, wq[...]).astype(BF)
    loads["wk"].wait()
    keys = dot(normed_in, wk[...]).astype(BF).astype(F32) * 128.0 ** (-0.5)
    for name in ("w_in", "w_fg", "bias", "smax"):
        loads[name].wait()
    gate_in = along(normed_in, w_in[...])
    forget = along(normed_in, w_fg[...]) + bias[...]
    forget = jnp.minimum(forget, 0.0) - jnp.log(1.0 + jnp.exp(-jnp.abs(forget)))
    head8 = iota((32, 8), 1)
    keeps, writes, floors = [], [], []
    for h in range(2):
        mine = head8 == 2 * x + h
        in_gate = jnp.sum(jnp.where(mine, gate_in, 0.0), axis=1, keepdims=True)
        carried = jnp.sum(jnp.where(mine, forget, 0.0), axis=1, keepdims=True) + as_column(smax[h : h + 1, :])
        new_max = jnp.maximum(carried, in_gate)
        keeps.append(jnp.exp(carried - new_max))
        writes.append(jnp.exp(in_gate - new_max))
        floors.append(jnp.exp(-new_max))
        max_out[h : h + 1, :] = as_row(new_max)
    loads["wv"].wait()
    value = dot(normed_in, wv[...]).astype(BF).astype(F32)
    loads["wo"].wait()
    out_gate = dot(normed_in, wo[...]).astype(BF).astype(F32)

    pl.semaphore_wait(barrier, 34)
    loads["gate"].wait()
    weight_out = first_round(gate_w, 0)

    eye = same.astype(BF)
    loads["st"].wait()
    loads["snorm"].wait()
    mixed, written_t = [], []
    for h in range(2):
        lanes = slice(h * 128, (h + 1) * 128)
        query_t = lax.dot_general(
            query[:, lanes], eye, (((0,), (0,)), ((), ())), preferred_element_type=F32
        )
        for s in range(32):
            numer[h, s : s + 1, :] = jnp.sum(
                query_t[:, s : s + 1] * st[s * 2 + h], axis=0, keepdims=True
            )
        q = query[:, lanes].astype(F32)
        written = writes[h] * keys[:, lanes]
        new_norm = keeps[h] * snorm[:, h, :] + written
        top = keeps[h] * numer[h] + jnp.sum(q * written, axis=1, keepdims=True) * value[:, lanes]
        denom = jnp.sum(q * new_norm, axis=1, keepdims=True)
        read = top / jnp.maximum(jnp.abs(denom), floors[h])
        mixed.append((read / (1.0 + jnp.exp(-out_gate[:, lanes]))).astype(BF))
        written_t.append(jnp.transpose(written))
        norm_out[h] = new_norm
    loads["wm"].wait()
    share = [
        (dot(mixed[0], wm[0:128, q * CH : (q + 1) * CH]) + dot(mixed[1], wm[128:256, q * CH : (q + 1) * CH])).astype(BF)
        for q in range(4)
    ]

    order = one_hot(128, 128, lambda r: ((r >> 3) & 3) * 32 + (r >> 5) * 8 + (r & 7))
    bsend[...] = dot(order, jnp.concatenate(share, axis=0)).astype(BF).reshape(4, 32, CH)
    brecv[x] = bsend[x]
    branch_out = []
    for d in (2, 1, 3):
        to = (x + d) % 4
        branch_out.append(remote(bsend.at[to], brecv.at[x], b_sem.at[0], b_sem.at[1], ep, to))
        branch_out[-1].start()

    weight_out += first_round(gate_w, 1)
    hperm[...] = dot(order, stacked(hidden)).reshape(4, 32, CH)

    for name in ("mix", "routes", "scores"):
        loads[name].wait()
    expert0, expert1 = as_column(routes[0:1, :].astype(F32)), as_column(routes[1:2, :].astype(F32))
    lane32 = iota((32, 32), 1)
    lane32_f = lane32.astype(F32)
    hot0 = (lane32_f == expert0).astype(F32)
    hot1 = (lane32_f == expert1).astype(F32)
    earlier = (iota((32, 32), 0) > lane32).astype(BF)
    before = dot(earlier, (hot0 + hot1).astype(BF))
    score0, score1 = as_column(scores[0:1, :]), as_column(scores[1:2, :])
    whole = score0 + score1

    def by_piece(column, step):
        return jnp.concatenate(
            [column[xx * 8 : xx * 8 + 8] + q * step for xx in range(4) for q in range(4)], axis=0
        )

    for k, (expert, hot, score) in enumerate(((expert0, hot0, score0), (expert1, hot1, score1))):
        rank = jnp.sum(hot * before, axis=1, keepdims=True)
        place = by_piece((expert * 16.0 + rank).astype(I32), 4)
        gk[k] = (iota((128, 512), 1) == place).astype(BF)
        share_s[k] = jnp.broadcast_to(by_piece(score / whole, 0.0), (128, 128))
    pm[...] = one_hot(512, 512, lambda r: ((r >> 2) & 31) * 16 + (r >> 7) * 4 + (r & 3))
    pmi[...] = one_hot(512, 512, lambda r: ((r >> 2) & 3) * 128 + (r >> 4) * 4 + (r & 3))
    pd[...] = one_hot(512, 512, lambda r: ((r >> 3) & 15) * 32 + (r >> 7) * 8 + (r & 7))
    pdi[...] = one_hot(512, 512, lambda r: ((r >> 3) & 3) * 128 + (r >> 5) * 8 + (r & 7))

    def gain(k):
        return jnp.concatenate(
            [jnp.broadcast_to(gains[k : k + 1, q * CH : (q + 1) * CH], (8, CH)) for q in range(4)],
            axis=0,
        )

    mix_rows = jnp.concatenate(
        [jnp.broadcast_to(mix[0:1, q * CH : (q + 1) * CH], (8, CH)) for q in range(4)], axis=0
    )

    for h in range(2):
        for s in range(32):
            matrix[s, h] = (
                keeps[h][s : s + 1, :] * st[s * 2 + h]
                + written_t[h][:, s : s + 1] * value[s : s + 1, h * 128 : (h + 1) * 128]
            )

    landed(brecv.at[pl.ds(0, 3)], b_sem.at[1])
    branch = brecv[0].astype(F32) + brecv[1].astype(F32) + brecv[2].astype(F32) + brecv[3].astype(F32)
    branch = branch.astype(BF).astype(F32)
    residual_f = hperm[x] + gain(1) * branch * lax.rsqrt(row_total(branch * branch) / 2048.0 + EPS)
    scale_two = lax.rsqrt(row_total(residual_f * residual_f) / 2048.0 + EPS)
    normed = (residual_f * scale_two * gain(2)).astype(BF)
    nall[x] = normed
    tok[p] = normed

    token_out = []
    for d in (2, 1, 3):
        to = (x + d) % 4
        token_out.append(remote(nall.at[x], nall.at[x], n_sem.at[0], n_sem.at[1], ep, to))
        token_out[-1].start()

    for chip in chips:
        remote(nall.at[x], tok.at[p], t_sem.at[0], t_sem.at[1], chip + c, x).start()
    loads["up"].wait()
    loads["down"].wait()
    weight_out += first_round(up_w, 0) + first_round(up_w, 1)
    weight_out += second_round(gate_w)
    resid_s[...] = residual_f.astype(BF).astype(F32)
    mix_dot = scale_two * row_total(residual_f * gain(2) * mix_rows)
    mixg_s[...] = jnp.broadcast_to(1.0 / (1.0 + jnp.exp(-mix_dot)), (32, 128))

    landed(nall.at[pl.ds(0, 3)], n_sem.at[1])
    chosen = gk[0] + gk[1]
    rows = lax.dot_general(
        chosen, nall[...].reshape(128, CH), (((0,), (0,)), ((), ())), preferred_element_type=F32
    )
    osend[...] = rows.astype(BF).reshape(32, 16, CH)
    orecv[ep] = osend[ep]

    for peer in peers:
        remote(osend.at[peer], orecv.at[ep], o_sem.at[0], o_sem.at[1], peer, x).start()
    weight_out += near_to_mate(gate_w)
    weight_out += second_round(up_w)
    weight_out += first_round(down_w, 0) + first_round(down_w, 1)
    weight_out += near_to_mate(up_w)
    weight_out += far_to_mate(gate_w)
    weight_out += far_to_mate(up_w)

    landed(tok.at[pl.ds(0, 15)], t_sem.at[1])
    xd[...] = dot(pd[...], tok[...].reshape(512, CH)).astype(BF).reshape(4, 128, CH)
    from_mate(gate_w)
    from_mate(up_w)
    for core in range(2):
        pre_gate = along(xd[0], gbuf[core, 0])
        pre_up = along(xd[0], ubuf[core, 0])
        for q in range(1, 4):
            pre_gate += along(xd[q], gbuf[core, q])
            pre_up += along(xd[q], ubuf[core, q])
        hden[core] = (silu(pre_gate) * pre_up).astype(BF)
    weight_out += second_round(down_w)
    weight_out += near_to_mate(down_w)

    landed(orecv.at[pl.ds(0, 31)], o_sem.at[1])
    xs[...] = dot(pm[...], orecv[...].reshape(512, CH)).astype(BF).reshape(4, 128, CH)
    loads["eg"].wait()
    loads["eu"].wait()
    gate_pre = dot(xs[0], wg[0])
    up_pre = dot(xs[0], wu[0])
    for q in range(1, 4):
        gate_pre += dot(xs[q], wg[q])
        up_pre += dot(xs[q], wu[q])
    hexp[...] = (silu(gate_pre) * up_pre).astype(BF)
    loads["ed"].wait()
    for q in range(4):
        ys[q * 128 : (q + 1) * 128] = dot(hexp[...], wd[:, q * CH : (q + 1) * CH]).astype(BF)
    rsend[...] = dot(pmi[...], ys[...]).astype(BF).reshape(32, 16, CH)
    rrecv[ep] = rsend[ep]

    for peer in peers:
        remote(rsend.at[peer], rrecv.at[ep], r_sem.at[0], r_sem.at[1], peer, x).start()

    weight_out += far_to_mate(down_w)
    from_mate(down_w)
    for q in range(4):
        yd[q * 128 : (q + 1) * 128] = (
            dot(hden[0], dbuf[0, q]) + dot(hden[1], dbuf[1, q])
        ).astype(BF)
    dsend[...] = dot(pdi[...], yd[...]).astype(BF).reshape(16, 32, CH)
    drecv[p] = dsend[p]

    for chip, place in zip(chips, places):
        remote(dsend.at[place], drecv.at[p], d_sem.at[0], d_sem.at[1], chip + c, x).start()

    landed(rrecv.at[pl.ds(0, 31)], r_sem.at[1])
    back = rrecv[...].reshape(512, CH)
    moe = share_s[0][:, 0:1] * dot(gk[0], back) + share_s[1][:, 0:1] * dot(gk[1], back)
    msend[...] = moe.astype(BF).reshape(4, 32, CH)
    mrecv[x] = msend[x]
    moe_out = []
    for d in (2, 1, 3):
        to = (x + d) % 4
        moe_out.append(remote(msend.at[to], mrecv.at[x], m_sem.at[0], m_sem.at[1], ep, to))
        moe_out[-1].start()

    landed(drecv.at[pl.ds(0, 15)], d_sem.at[1])
    dense = drecv[0].astype(F32)
    for n in range(1, 16):
        dense += drecv[n].astype(F32)
    landed(mrecv.at[pl.ds(0, 3)], m_sem.at[1])
    ffn = mrecv[0].astype(F32) + mrecv[1].astype(F32) + mrecv[2].astype(F32) + mrecv[3].astype(F32)
    ffn += mixg_s[:, 0:1] * dense
    scale_ffn = lax.rsqrt(row_total(ffn * ffn) / 2048.0 + EPS)
    fsend[...] = (resid_s[...] + gain(3) * ffn * scale_ffn).reshape(4, 8, CH)
    frecv[x] = fsend[x]
    last_out = []
    for d in (2, 1, 3):
        to = (x + d) % 4
        last_out.append(remote(fsend.at[to], frecv.at[x], f_sem.at[0], f_sem.at[1], ep, to))
        last_out[-1].start()

    for copy in weight_out:
        copy.wait_send()
    landed(bsend.at[pl.ds(0, 3)], b_sem.at[0])
    landed(nall.at[pl.ds(0, 3)], n_sem.at[0])
    landed(tok.at[pl.ds(0, 15)], t_sem.at[0])
    landed(osend.at[pl.ds(0, 31)], o_sem.at[0])
    landed(rsend.at[pl.ds(0, 31)], r_sem.at[0])
    landed(dsend.at[pl.ds(0, 15)], d_sem.at[0])
    landed(msend.at[pl.ds(0, 3)], m_sem.at[0])
    landed(frecv.at[pl.ds(0, 3)], f_sem.at[1])
    out[...] = frecv[...].reshape(32, CH).astype(BF)
    landed(fsend.at[pl.ds(0, 3)], f_sem.at[0])


def whole(*arrays):
    V = pltpu.VMEM
    dma = pltpu.SemaphoreType.DMA
    vm = pl.BlockSpec(memory_space=pltpu.VMEM)
    hb = pl.BlockSpec(memory_space=pltpu.HBM)
    return pl.pallas_call(
        whole_kernel,
        out_shape=(
            V((32, CH), BF), V((32, 2, 128, 128), F32), V((2, 32, 128), F32), V((2, 32), F32),
        ),
        in_specs=[hb] * len(arrays),
        out_specs=(vm,) * 4,
        scratch_shapes=[
            V((32, 2048), BF), V((4, 2048), F32), V((1, 2048), F32), V((2, 32), I32), V((2, 32), F32),
            V((8, 2048), BF), V((8, 2048), BF), V((1, 8), F32), V((2, 32), F32), V((32, 2, 128), F32),
            V((2048, 256), BF), V((2048, 256), BF), V((2048, 256), BF), V((2048, 256), BF),
            V((256, 2048), BF), V((64, 128, 128), F32), V((2, 32, 128), F32),
            V((4, 512, 896), BF), V((4, 512, 896), BF), V((896, 2048), BF),
            V((2, 4, 176, 512), BF), V((2, 4, 176, 512), BF), V((2, 4, 176, 512), BF),
            V((4, 32, CH), BF), V((4, 32, CH), BF), V((4, 32, CH), F32), V((4, 32, CH), BF),
            V((16, 32, CH), BF),
            V((32, 16, CH), BF), V((32, 16, CH), BF), V((32, 16, CH), BF), V((32, 16, CH), BF),
            V((16, 32, CH), BF), V((16, 32, CH), BF),
            V((4, 32, CH), BF), V((4, 32, CH), BF), V((4, 8, CH), F32), V((4, 8, CH), F32),
            V((512, 512), BF), V((512, 512), BF), V((512, 512), BF), V((512, 512), BF),
            V((2, 128, 512), BF), V((4, 128, CH), BF), V((4, 128, CH), BF),
            V((512, CH), BF), V((512, CH), BF), V((128, 896), BF), V((2, 128, 176), BF),
            V((32, CH), F32), V((32, 128), F32), V((2, 128, 128), F32),
            dma((22,)), dma((2,)), dma((2,)), dma((2,)), dma((2,)), dma((2,)), dma((2,)),
            dma((2,)), dma((2,)),
            dma((11,)), dma((11,)), dma((11,)), dma((11,)), dma((11,)), dma((11,)),
        ],
        compiler_params=pltpu.CompilerParams(
            collective_id=0, has_side_effects=True, vmem_limit_bytes=44 * 1024 * 1024
        ),
        name="whole",
    )(*(pltpu.with_memory_space_constraint(a, pltpu.HBM) for a in arrays))


def memory_kernel(matrix, norm, top, hidden_in, norm_out, top_out, hidden_out, matrix_h, out_sem):
    stores = [
        pltpu.make_async_copy(matrix.at[pl.ds(n * 4, 4)], matrix_h.at[pl.ds(n * 4, 4)], out_sem.at[n])
        for n in range(8)
    ]
    for store in stores:
        store.start()
    for h in range(2):
        norm_out[:, h, :] = norm[h]
    top_out[...] = top[...]
    hidden_out[...] = hidden_in[...]
    for store in stores:
        store.wait()


def memory(matrix, norm, top, hidden_in):
    vm = pl.BlockSpec(memory_space=pltpu.VMEM)
    return pl.pallas_call(
        memory_kernel,
        out_shape=(
            jax.ShapeDtypeStruct((32, 2, 128), F32),
            jax.ShapeDtypeStruct((2, 32), F32),
            jax.ShapeDtypeStruct((32, CH), BF),
            pltpu.HBM((32, 2, 128, 128), F32),
        ),
        in_specs=[vm] * 4,
        out_specs=(vm, vm, vm, pl.BlockSpec(memory_space=pltpu.HBM)),
        scratch_shapes=[pltpu.SemaphoreType.DMA((8,))],
        compiler_params=pltpu.CompilerParams(vmem_limit_bytes=16 * 1024 * 1024),
        name="memory",
    )(matrix, norm, top, hidden_in)


def local(
    hidden,
    norm_gains,
    w_query,
    w_key,
    w_value,
    w_outgate,
    w_input_gate,
    w_forget_gate,
    forget_bias,
    w_mix_out,
    state_matrix,
    state_norm,
    state_max,
    routes,
    route_scores,
    expert_gate,
    expert_up,
    expert_down,
    dense_gate,
    dense_up,
    dense_down,
    dense_mix,
):
    new_hidden, matrix, norm, top = whole(
        hidden, norm_gains, dense_mix.reshape(1, -1), routes.T, route_scores.T,
        w_input_gate.T, w_forget_gate.T, forget_bias.reshape(1, -1), state_max.T, state_norm,
        w_query, w_key, w_value, w_outgate, w_mix_out, state_matrix.reshape(64, 128, 128),
        expert_gate.reshape(4, CH, -1), expert_up.reshape(4, CH, -1), expert_down[0],
        dense_gate.T, dense_up.T, dense_down,
    )
    new_norm, new_top, new_hidden, new_matrix = memory(matrix, norm, top, new_hidden)
    return (new_hidden, new_matrix, new_norm, new_top.T)


def solution(mesh):
    placed = (
        P("ep", None),
        P(),
        P(None, "tp"),
        P(None, "tp"),
        P(None, "tp"),
        P(None, "tp"),
        P(),
        P(),
        P(),
        P("tp", None),
        P("ep", "tp", None, None),
        P("ep", "tp", None),
        P("ep", "tp"),
        P("ep", None),
        P("ep", None),
        P("ep", None, "tp"),
        P("ep", None, "tp"),
        P("ep", "tp", None),
        P("tp", "ep"),
        P("tp", "ep"),
        P("ep", "tp"),
        P(),
    )
    return jax.shard_map(
        local,
        mesh=mesh,
        in_specs=placed,
        out_specs=(P("ep", "tp"), P("ep", "tp", None, None), P("ep", "tp", None), P("ep", "tp")),
        check_vma=False,
    )
```

time: 66.6 us -> 55.7 us (0.84)
  the two profiles are of different devices: /device:TPU:0 before, /device:TPU:24 now
where the time goes in v3:
time: 55.7 us; the launch traced here: 55.6 us
  Pallas kernels  54.9 us (99%)
  between operations  0.65 us (1%)
    pallas_call x1, Pallas kernels, whole(): pl.pallas_call(whole_kernel, out_shape=(V((32, CH), BF), V((32, 2, 128, 1...  52.2 us
    pallas_call x1, Pallas kernels, memory(): pl.pallas_call(memory_kernel, out_shape=(jax.ShapeDtypeStruct((32, 2, 128...  2.7 us

profile of v3, /device:TPU:24, one launch (start us, length us, event | category | flops | bytes accessed | tf_op | source)
XLA Modules:
  0.0 55.6 jit_solution(7546555443926382970)
XLA Ops:
  0.6 52.2 %whole.1 = (bf16[32,512]{1,0:T(8,128)(2,1)S(1)}, f32[32,2,128,128]{3,2,1,0:T(8,128)S(1)}, f32[2,32,128]{2,1,0:T(8,128)S(1)}, f32[2,32]{1,0:T(2,128)S(1)}) custom-call(bf16[32,2048]{1,0:T(8,128)(2,1)} %hidden_h.1, f32[4,2048]{1,0:T(4,128)} %gains_h.1, f32[1,2048]{1,0:T(1,128)} %bitcast.22, s32[2,32]{1,0:T(2,128)} %bitcast.23, f32[2,32]{1,0:T(2,128)} %bitcast.24, ...), custom_call_target="tpu_custom_call" | custom-call | tf_op jit(solution)/shard_map/whole/pallas_call | solution.py:429
  52.9 2.7 %memory.1 = (f32[32,2,128]{2,1,0:T(2,128)}, f32[2,32]{1,0:T(2,128)}, bf16[32,512]{1,0:T(8,128)(2,1)}, f32[32,2,128,128]{3,2,1,0:T(8,128)}) custom-call(f32[32,2,128,128]{3,2,1,0:T(8,128)S(1)} %get-tuple-element.12.matrix, f32[2,32,128]{2,1,0:T(8,128)S(1)} %get-tuple-element.13.norm, f32[2,32]{1,0:T(2,128)S(1)} %get-tuple-element.14.top, ...), custom_call_target="tpu_custom_call" | custom-call | tf_op jit(solution)/shard_map/memory/pallas_call | solution.py:480

commit v4 on v3

--- a/solution.py
+++ b/solution.py
@@ -14,6 +14,7 @@
     ((dz, dy) for dz in range(4) for dy in range(4) if dz or dy),
     key=lambda s: -(min(s[0], 4 - s[0]) + min(s[1], 4 - s[1])),
 )
+EARLY = 7
 PIECES = ((0, 96), (96, 80))
 CH = 512
 
@@ -51,7 +52,7 @@
     hidden, gains, mix, routes, scores, w_in, w_fg, bias, smax, snorm,
     wq, wk, wv, wo, wm, st, numer,
     wg, wu, wd, gbuf, ubuf, dbuf,
-    bsend, brecv, hperm, nall, tok, osend, orecv, rsend, rrecv, dsend, drecv,
+    bsend, brecv, hperm, nall, tok, osend, orecv, rsend, rrecv, dsend, drecv, dsum,
     msend, mrecv, fsend, frecv,
     pm, pmi, pd, pdi, gk, xs, xd, ys, yd, hexp, hden, resid_s, mixg_s, share_s,
     load_sem, b_sem, n_sem, t_sem, o_sem, r_sem, d_sem, m_sem, f_sem,
@@ -71,8 +72,9 @@
     core_at = [c, 1 - c]
     places = [((z + dz) % 4) * 4 + (y + dy) % 4 for dz, dy in CHIP_STEPS]
     chips = [z_at[dz] + y_at[dy] for dz, dy in CHIP_STEPS]
-    peers = [base + core for base in chips for core in core_at]
-    peers.append(p * 2 + core_at[1])
+    peers = [p * 2 + core_at[1]]
+    for n, base in enumerate(chips):
+        peers += [base + core_at[n % 2], base + core_at[1 - n % 2]]
 
     def remote(src, dst, ssem, rsem, to_ep, to_x):
         return pltpu.make_async_remote_copy(
@@ -92,7 +94,8 @@
                 ("hidden", hidden_h, hidden), ("gains", gains_h, gains),
                 ("wq", wq_h, wq), ("wk", wk_h, wk), ("w_in", w_in_h, w_in), ("w_fg", w_fg_h, w_fg),
                 ("bias", bias_h, bias), ("smax", smax_h, smax), ("wv", wv_h, wv), ("wo", wo_h, wo),
-                ("gate", dg, gbuf.at[c, x]), ("st", st_h, st), ("snorm", snorm_h, snorm), ("wm", wm_h, wm),
+                ("gate", dg, gbuf.at[c, x]), ("st0", st_h.at[pl.ds(0, 32)], st.at[pl.ds(0, 32)]),
+                ("st1", st_h.at[pl.ds(32, 32)], st.at[pl.ds(32, 32)]), ("snorm", snorm_h, snorm), ("wm", wm_h, wm),
                 ("up", du, ubuf.at[c, x]), ("down", dd, dbuf.at[c, x]), ("mix", mix_h, mix),
                 ("routes", routes_h, routes), ("scores", scores_h, scores),
                 ("eg", eg, wg), ("eu", eu, wu), ("ed", ed, wd),
@@ -181,8 +184,8 @@
         return lax.dot_general(a, b, (((1,), (1,)), ((), ())), preferred_element_type=F32)
 
     loads["wq"].wait()
+    loads["wk"].wait()
     query = dot(normed_in, wq[...]).astype(BF)
-    loads["wk"].wait()
     keys = dot(normed_in, wk[...]).astype(BF).astype(F32) * 128.0 ** (-0.5)
     for name in ("w_in", "w_fg", "bias", "smax"):
         loads[name].wait()
@@ -201,8 +204,8 @@
         floors.append(jnp.exp(-new_max))
         max_out[h : h + 1, :] = as_row(new_max)
     loads["wv"].wait()
+    loads["wo"].wait()
     value = dot(normed_in, wv[...]).astype(BF).astype(F32)
-    loads["wo"].wait()
     out_gate = dot(normed_in, wo[...]).astype(BF).astype(F32)
 
     pl.semaphore_wait(barrier, 34)
@@ -210,18 +213,25 @@
     weight_out = first_round(gate_w, 0)
 
     eye = same.astype(BF)
-    loads["st"].wait()
+    queries_t = [
+        lax.dot_general(
+            query[:, h * 128 : (h + 1) * 128], eye, (((0,), (0,)), ((), ())), preferred_element_type=F32
+        ).astype(BF)
+        for h in range(2)
+    ]
+    for half in range(2):
+        loads[("st0", "st1")[half]].wait()
+        for h in range(2):
+            for s in range(16 * half, 16 * half + 16, 2):
+                wide = dot(queries_t[h], (iota((32, 256), 0) == s + (iota((32, 256), 1) >> 7)).astype(BF))
+                numer[h, s : s + 1, :] = jnp.sum(wide[:, 0:128] * st[s * 2 + h], axis=0, keepdims=True)
+                numer[h, s + 1 : s + 2, :] = jnp.sum(
+                    wide[:, 128:256] * st[s * 2 + 2 + h], axis=0, keepdims=True
+                )
     loads["snorm"].wait()
     mixed, written_t = [], []
     for h in range(2):
         lanes = slice(h * 128, (h + 1) * 128)
-        query_t = lax.dot_general(
-            query[:, lanes], eye, (((0,), (0,)), ((), ())), preferred_element_type=F32
-        )
-        for s in range(32):
-            numer[h, s : s + 1, :] = jnp.sum(
-                query_t[:, s : s + 1] * st[s * 2 + h], axis=0, keepdims=True
-            )
         q = query[:, lanes].astype(F32)
         written = writes[h] * keys[:, lanes]
         new_norm = keeps[h] * snorm[:, h, :] + written
@@ -230,7 +240,7 @@
         read = top / jnp.maximum(jnp.abs(denom), floors[h])
         mixed.append((read / (1.0 + jnp.exp(-out_gate[:, lanes]))).astype(BF))
         written_t.append(jnp.transpose(written))
-        norm_out[h] = new_norm
+        norm_out[:, h, :] = new_norm
     loads["wm"].wait()
     share = [
         (dot(mixed[0], wm[0:128, q * CH : (q + 1) * CH]) + dot(mixed[1], wm[128:256, q * CH : (q + 1) * CH])).astype(BF)
@@ -274,7 +284,7 @@
     pm[...] = one_hot(512, 512, lambda r: ((r >> 2) & 31) * 16 + (r >> 7) * 4 + (r & 3))
     pmi[...] = one_hot(512, 512, lambda r: ((r >> 2) & 3) * 128 + (r >> 4) * 4 + (r & 3))
     pd[...] = one_hot(512, 512, lambda r: ((r >> 3) & 15) * 32 + (r >> 7) * 8 + (r & 7))
-    pdi[...] = one_hot(512, 512, lambda r: ((r >> 3) & 3) * 128 + (r >> 5) * 8 + (r & 7))
+    pdi[...] = one_hot(256, 256, lambda r: ((r >> 3) & 1) * 128 + (r >> 4) * 8 + (r & 7))
 
     def gain(k):
         return jnp.concatenate(
@@ -308,12 +318,10 @@
         token_out.append(remote(nall.at[x], nall.at[x], n_sem.at[0], n_sem.at[1], ep, to))
         token_out[-1].start()
 
-    for chip in chips:
+    for chip in chips[:EARLY]:
         remote(nall.at[x], tok.at[p], t_sem.at[0], t_sem.at[1], chip + c, x).start()
     loads["up"].wait()
     loads["down"].wait()
-    weight_out += first_round(up_w, 0) + first_round(up_w, 1)
-    weight_out += second_round(gate_w)
     resid_s[...] = residual_f.astype(BF).astype(F32)
     mix_dot = scale_two * row_total(residual_f * gain(2) * mix_rows)
     mixg_s[...] = jnp.broadcast_to(1.0 / (1.0 + jnp.exp(-mix_dot)), (32, 128))
@@ -328,26 +336,14 @@
 
     for peer in peers:
         remote(osend.at[peer], orecv.at[ep], o_sem.at[0], o_sem.at[1], peer, x).start()
+    weight_out += first_round(up_w, 0) + first_round(up_w, 1)
+    weight_out += second_round(gate_w)
+    for chip in chips[EARLY:]:
+        remote(nall.at[x], tok.at[p], t_sem.at[0], t_sem.at[1], chip + c, x).start()
     weight_out += near_to_mate(gate_w)
     weight_out += second_round(up_w)
     weight_out += first_round(down_w, 0) + first_round(down_w, 1)
     weight_out += near_to_mate(up_w)
-    weight_out += far_to_mate(gate_w)
-    weight_out += far_to_mate(up_w)
-
-    landed(tok.at[pl.ds(0, 15)], t_sem.at[1])
-    xd[...] = dot(pd[...], tok[...].reshape(512, CH)).astype(BF).reshape(4, 128, CH)
-    from_mate(gate_w)
-    from_mate(up_w)
-    for core in range(2):
-        pre_gate = along(xd[0], gbuf[core, 0])
-        pre_up = along(xd[0], ubuf[core, 0])
-        for q in range(1, 4):
-            pre_gate += along(xd[q], gbuf[core, q])
-            pre_up += along(xd[q], ubuf[core, q])
-        hden[core] = (silu(pre_gate) * pre_up).astype(BF)
-    weight_out += second_round(down_w)
-    weight_out += near_to_mate(down_w)
 
     landed(orecv.at[pl.ds(0, 31)], o_sem.at[1])
     xs[...] = dot(pm[...], orecv[...].reshape(512, CH)).astype(BF).reshape(4, 128, CH)
@@ -359,6 +355,7 @@
         gate_pre += dot(xs[q], wg[q])
         up_pre += dot(xs[q], wu[q])
     hexp[...] = (silu(gate_pre) * up_pre).astype(BF)
+    weight_out += far_to_mate(gate_w)
     loads["ed"].wait()
     for q in range(4):
         ys[q * 128 : (q + 1) * 128] = dot(hexp[...], wd[:, q * CH : (q + 1) * CH]).astype(BF)
@@ -368,17 +365,45 @@
     for peer in peers:
         remote(rsend.at[peer], rrecv.at[ep], r_sem.at[0], r_sem.at[1], peer, x).start()
 
+    weight_out += far_to_mate(up_w)
+    weight_out += second_round(down_w)
+
+    landed(tok.at[pl.ds(0, 15)], t_sem.at[1])
+    xd[...] = dot(pd[...], tok[...].reshape(512, CH)).astype(BF).reshape(4, 128, CH)
+    weight_out += near_to_mate(down_w)
+    from_mate(gate_w)
+    from_mate(up_w)
+    for core in range(2):
+        pre_gate = along(xd[0], gbuf[core, 0])
+        pre_up = along(xd[0], ubuf[core, 0])
+        for q in range(1, 4):
+            pre_gate += along(xd[q], gbuf[core, q])
+            pre_up += along(xd[q], ubuf[core, q])
+        hden[core] = (silu(pre_gate) * pre_up).astype(BF)
+
+    def dense_half(half):
+        for n in (2 * half, 2 * half + 1):
+            yd[n * 128 : (n + 1) * 128] = (
+                dot(hden[0], dbuf[0, quarters[n]]) + dot(hden[1], dbuf[1, quarters[n]])
+            ).astype(BF)
+        rows = dot(pdi[...], yd[half * 256 : (half + 1) * 256])
+        dsend[half] = rows.astype(BF).reshape(16, 16, CH)
+        drecv[half, p] = dsend[half, p]
+        for chip, place in zip(chips, places):
+            remote(
+                dsend.at[half, place], drecv.at[half, p],
+                d_sem.at[2 * half], d_sem.at[2 * half + 1], chip + c, x,
+            ).start()
+
+    quarters = (x, left, right, far)
+    landed(dbuf.at[1 - c, x], dr_sem.at[6])
+    landed(dbuf.at[1 - c, left], dr_sem.at[7])
+    dense_half(0)
     weight_out += far_to_mate(down_w)
-    from_mate(down_w)
-    for q in range(4):
-        yd[q * 128 : (q + 1) * 128] = (
-            dot(hden[0], dbuf[0, q]) + dot(hden[1], dbuf[1, q])
-        ).astype(BF)
-    dsend[...] = dot(pdi[...], yd[...]).astype(BF).reshape(16, 32, CH)
-    drecv[p] = dsend[p]
-
-    for chip, place in zip(chips, places):
-        remote(dsend.at[place], drecv.at[p], d_sem.at[0], d_sem.at[1], chip + c, x).start()
+    landed(dbuf.at[1 - c, right], dr_sem.at[8])
+    for piece in range(2):
+        landed(dbuf.at[1 - c, far, pl.ds(*PIECES[piece])], dr_sem.at[9 + piece])
+    dense_half(1)
 
     landed(rrecv.at[pl.ds(0, 31)], r_sem.at[1])
     back = rrecv[...].reshape(512, CH)
@@ -391,10 +416,14 @@
         moe_out.append(remote(msend.at[to], mrecv.at[x], m_sem.at[0], m_sem.at[1], ep, to))
         moe_out[-1].start()
 
-    landed(drecv.at[pl.ds(0, 15)], d_sem.at[1])
-    dense = drecv[0].astype(F32)
-    for n in range(1, 16):
-        dense += drecv[n].astype(F32)
+    for half in range(2):
+        landed(drecv.at[half, pl.ds(0, 15)], d_sem.at[2 * half + 1])
+        total = drecv[half, 0].astype(F32)
+        for n in range(1, 16):
+            total += drecv[half, n].astype(F32)
+        dsum[quarters[2 * half]] = total[0:8]
+        dsum[quarters[2 * half + 1]] = total[8:16]
+    dense = dsum[...].reshape(32, CH)
     landed(mrecv.at[pl.ds(0, 3)], m_sem.at[1])
     ffn = mrecv[0].astype(F32) + mrecv[1].astype(F32) + mrecv[2].astype(F32) + mrecv[3].astype(F32)
     ffn += mixg_s[:, 0:1] * dense
@@ -414,7 +443,8 @@
     landed(tok.at[pl.ds(0, 15)], t_sem.at[0])
     landed(osend.at[pl.ds(0, 31)], o_sem.at[0])
     landed(rsend.at[pl.ds(0, 31)], r_sem.at[0])
-    landed(dsend.at[pl.ds(0, 15)], d_sem.at[0])
+    landed(dsend.at[0, pl.ds(0, 15)], d_sem.at[0])
+    landed(dsend.at[1, pl.ds(0, 15)], d_sem.at[2])
     landed(msend.at[pl.ds(0, 3)], m_sem.at[0])
     landed(frecv.at[pl.ds(0, 3)], f_sem.at[1])
     out[...] = frecv[...].reshape(32, CH).astype(BF)
@@ -429,7 +459,7 @@
     return pl.pallas_call(
         whole_kernel,
         out_shape=(
-            V((32, CH), BF), V((32, 2, 128, 128), F32), V((2, 32, 128), F32), V((2, 32), F32),
+            V((32, CH), BF), V((32, 2, 128, 128), F32), V((32, 2, 128), F32), V((2, 32), F32),
         ),
         in_specs=[hb] * len(arrays),
         out_specs=(vm,) * 4,
@@ -443,13 +473,13 @@
             V((4, 32, CH), BF), V((4, 32, CH), BF), V((4, 32, CH), F32), V((4, 32, CH), BF),
             V((16, 32, CH), BF),
             V((32, 16, CH), BF), V((32, 16, CH), BF), V((32, 16, CH), BF), V((32, 16, CH), BF),
-            V((16, 32, CH), BF), V((16, 32, CH), BF),
+            V((2, 16, 16, CH), BF), V((2, 16, 16, CH), BF), V((4, 8, CH), F32),
             V((4, 32, CH), BF), V((4, 32, CH), BF), V((4, 8, CH), F32), V((4, 8, CH), F32),
-            V((512, 512), BF), V((512, 512), BF), V((512, 512), BF), V((512, 512), BF),
+            V((512, 512), BF), V((512, 512), BF), V((512, 512), BF), V((256, 256), BF),
             V((2, 128, 512), BF), V((4, 128, CH), BF), V((4, 128, CH), BF),
             V((512, CH), BF), V((512, CH), BF), V((128, 896), BF), V((2, 128, 176), BF),
             V((32, CH), F32), V((32, 128), F32), V((2, 128, 128), F32),
-            dma((22,)), dma((2,)), dma((2,)), dma((2,)), dma((2,)), dma((2,)), dma((2,)),
+            dma((23,)), dma((2,)), dma((2,)), dma((2,)), dma((2,)), dma((2,)), dma((4,)),
             dma((2,)), dma((2,)),
             dma((11,)), dma((11,)), dma((11,)), dma((11,)), dma((11,)), dma((11,)),
         ],
@@ -460,37 +490,30 @@
     )(*(pltpu.with_memory_space_constraint(a, pltpu.HBM) for a in arrays))
 
 
-def memory_kernel(matrix, norm, top, hidden_in, norm_out, top_out, hidden_out, matrix_h, out_sem):
+def memory_kernel(matrix, norm, top, last, matrix_h, norm_h, top_h, last_h, sem):
     stores = [
-        pltpu.make_async_copy(matrix.at[pl.ds(n * 4, 4)], matrix_h.at[pl.ds(n * 4, 4)], out_sem.at[n])
+        pltpu.make_async_copy(matrix.at[pl.ds(n * 4, 4)], matrix_h.at[pl.ds(n * 4, 4)], sem.at[n])
         for n in range(8)
     ]
+    for n, (src, dst) in enumerate(((norm, norm_h), (top, top_h), (last, last_h))):
+        stores.append(pltpu.make_async_copy(src, dst, sem.at[8 + n]))
     for store in stores:
         store.start()
-    for h in range(2):
-        norm_out[:, h, :] = norm[h]
-    top_out[...] = top[...]
-    hidden_out[...] = hidden_in[...]
     for store in stores:
         store.wait()
 
 
-def memory(matrix, norm, top, hidden_in):
-    vm = pl.BlockSpec(memory_space=pltpu.VMEM)
+def memory(matrix, norm, top, last):
+    arrays = (matrix, norm, top, last)
     return pl.pallas_call(
         memory_kernel,
-        out_shape=(
-            jax.ShapeDtypeStruct((32, 2, 128), F32),
-            jax.ShapeDtypeStruct((2, 32), F32),
-            jax.ShapeDtypeStruct((32, CH), BF),
-            pltpu.HBM((32, 2, 128, 128), F32),
-        ),
-        in_specs=[vm] * 4,
-        out_specs=(vm, vm, vm, pl.BlockSpec(memory_space=pltpu.HBM)),
-        scratch_shapes=[pltpu.SemaphoreType.DMA((8,))],
+        out_shape=tuple(pltpu.HBM(a.shape, a.dtype) for a in arrays),
+        in_specs=[pl.BlockSpec(memory_space=pltpu.VMEM)] * 4,
+        out_specs=(pl.BlockSpec(memory_space=pltpu.HBM),) * 4,
+        scratch_shapes=[pltpu.SemaphoreType.DMA((11,))],
         compiler_params=pltpu.CompilerParams(vmem_limit_bytes=16 * 1024 * 1024),
         name="memory",
-    )(matrix, norm, top, hidden_in)
+    )(*arrays)
 
 
 def local(
@@ -524,7 +547,7 @@
         expert_gate.reshape(4, CH, -1), expert_up.reshape(4, CH, -1), expert_down[0],
         dense_gate.T, dense_up.T, dense_down,
     )
-    new_norm, new_top, new_hidden, new_matrix = memory(matrix, norm, top, new_hidden)
+    new_matrix, new_norm, new_top, new_hidden = memory(matrix, norm, top, new_hidden)
     return (new_hidden, new_matrix, new_norm, new_top.T)
 
 

time: 55.7 us -> 52 us (0.934)
  the two profiles are of different devices: /device:TPU:24 before, /device:TPU:0 now
where the time goes in v4:
time: 52 us; the launch traced here: 51.8 us
  Pallas kernels  51.1 us (98%)
  between operations  0.65 us (1%)
    pallas_call x1, Pallas kernels, whole(): pl.pallas_call(whole_kernel, out_shape=(V((32, CH), BF), V((32, 2, 128, 1...  49 us
    pallas_call x1, Pallas kernels, memory(): pl.pallas_call(memory_kernel, out_shape=tuple((pltpu.HBM(a.shape, a.dtype...  2.11 us

profile of v4, /device:TPU:0, one launch (start us, length us, event | category | flops | bytes accessed | tf_op | source)
XLA Modules:
  0.0 51.8 jit_solution(14745072538658001158)
XLA Ops:
  0.6 49.0 %whole.1 = (bf16[32,512]{1,0:T(8,128)(2,1)S(1)}, f32[32,2,128,128]{3,2,1,0:T(8,128)S(1)}, f32[32,2,128]{2,1,0:T(2,128)S(1)}, f32[2,32]{1,0:T(2,128)S(1)}) custom-call(bf16[32,2048]{1,0:T(8,128)(2,1)} %hidden_h.1, f32[4,2048]{1,0:T(4,128)} %gains_h.1, f32[1,2048]{1,0:T(1,128)} %bitcast.22, s32[2,32]{1,0:T(2,128)} %bitcast.23, f32[2,32]{1,0:T(2,128)} %bitcast.24, ...), custom_call_target="tpu_custom_call" | custom-call | tf_op jit(solution)/shard_map/whole/pallas_call | solution.py:459
  49.7 2.1 %memory.1 = (f32[32,2,128,128]{3,2,1,0:T(8,128)}, f32[32,2,128]{2,1,0:T(2,128)}, f32[2,32]{1,0:T(2,128)}, bf16[32,512]{1,0:T(8,128)(2,1)}) custom-call(f32[32,2,128,128]{3,2,1,0:T(8,128)S(1)} %get-tuple-element.12.matrix, f32[32,2,128]{2,1,0:T(2,128)S(1)} %get-tuple-element.13.norm, f32[2,32]{1,0:T(2,128)S(1)} %get-tuple-element.14.top, ...), custom_call_target="tpu_custom_call" | custom-call | tf_op jit(solution)/shard_map/memory/pallas_call | solution.py:508

commit v5 on v4

--- a/solution.py
+++ b/solution.py
@@ -54,7 +54,7 @@
     wg, wu, wd, gbuf, ubuf, dbuf,
     bsend, brecv, hperm, nall, tok, osend, orecv, rsend, rrecv, dsend, drecv, dsum,
     msend, mrecv, fsend, frecv,
-    pm, pmi, pd, pdi, gk, xs, xd, ys, yd, hexp, hden, resid_s, mixg_s, share_s,
+    pm, pmi, pd, chosen, gk, xs, xd, ys, hexp, hden, resid_s, mixg_s, share_s,
     load_sem, b_sem, n_sem, t_sem, o_sem, r_sem, d_sem, m_sem, f_sem,
     gs_sem, gr_sem, us_sem, ur_sem, ds_sem, dr_sem,
 ):
@@ -243,12 +243,12 @@
         norm_out[:, h, :] = new_norm
     loads["wm"].wait()
     share = [
-        (dot(mixed[0], wm[0:128, q * CH : (q + 1) * CH]) + dot(mixed[1], wm[128:256, q * CH : (q + 1) * CH])).astype(BF)
+        (dot(mixed[0], wm[0:128, q * CH : (q + 1) * CH]) + dot(mixed[1], wm[128:256, q * CH : (q + 1) * CH]))
         for q in range(4)
     ]
 
-    order = one_hot(128, 128, lambda r: ((r >> 3) & 3) * 32 + (r >> 5) * 8 + (r & 7))
-    bsend[...] = dot(order, jnp.concatenate(share, axis=0)).astype(BF).reshape(4, 32, CH)
+    for xx in range(4):
+        bsend[xx] = jnp.concatenate([part[xx * 8 : xx * 8 + 8] for part in share], axis=0).astype(BF)
     brecv[x] = bsend[x]
     branch_out = []
     for d in (2, 1, 3):
@@ -257,6 +257,7 @@
         branch_out[-1].start()
 
     weight_out += first_round(gate_w, 1)
+    order = one_hot(128, 128, lambda r: ((r >> 3) & 3) * 32 + (r >> 5) * 8 + (r & 7))
     hperm[...] = dot(order, stacked(hidden)).reshape(4, 32, CH)
 
     for name in ("mix", "routes", "scores"):
@@ -281,10 +282,10 @@
         place = by_piece((expert * 16.0 + rank).astype(I32), 4)
         gk[k] = (iota((128, 512), 1) == place).astype(BF)
         share_s[k] = jnp.broadcast_to(by_piece(score / whole, 0.0), (128, 128))
+    chosen[...] = jnp.transpose((gk[0] + gk[1]).astype(F32)).astype(BF)
     pm[...] = one_hot(512, 512, lambda r: ((r >> 2) & 31) * 16 + (r >> 7) * 4 + (r & 3))
     pmi[...] = one_hot(512, 512, lambda r: ((r >> 2) & 3) * 128 + (r >> 4) * 4 + (r & 3))
     pd[...] = one_hot(512, 512, lambda r: ((r >> 3) & 15) * 32 + (r >> 7) * 8 + (r & 7))
-    pdi[...] = one_hot(256, 256, lambda r: ((r >> 3) & 1) * 128 + (r >> 4) * 8 + (r & 7))
 
     def gain(k):
         return jnp.concatenate(
@@ -327,10 +328,7 @@
     mixg_s[...] = jnp.broadcast_to(1.0 / (1.0 + jnp.exp(-mix_dot)), (32, 128))
 
     landed(nall.at[pl.ds(0, 3)], n_sem.at[1])
-    chosen = gk[0] + gk[1]
-    rows = lax.dot_general(
-        chosen, nall[...].reshape(128, CH), (((0,), (0,)), ((), ())), preferred_element_type=F32
-    )
+    rows = dot(chosen[...], nall[...].reshape(128, CH))
     osend[...] = rows.astype(BF).reshape(32, 16, CH)
     orecv[ep] = osend[ep]
 
@@ -382,12 +380,12 @@
         hden[core] = (silu(pre_gate) * pre_up).astype(BF)
 
     def dense_half(half):
-        for n in (2 * half, 2 * half + 1):
-            yd[n * 128 : (n + 1) * 128] = (
-                dot(hden[0], dbuf[0, quarters[n]]) + dot(hden[1], dbuf[1, quarters[n]])
-            ).astype(BF)
-        rows = dot(pdi[...], yd[half * 256 : (half + 1) * 256])
-        dsend[half] = rows.astype(BF).reshape(16, 16, CH)
+        pair = [
+            dot(hden[0], dbuf[0, quarters[n]]) + dot(hden[1], dbuf[1, quarters[n]])
+            for n in (2 * half, 2 * half + 1)
+        ]
+        for n in range(16):
+            dsend[half, n] = jnp.concatenate([part[n * 8 : n * 8 + 8] for part in pair], axis=0).astype(BF)
         drecv[half, p] = dsend[half, p]
         for chip, place in zip(chips, places):
             remote(
@@ -475,9 +473,9 @@
             V((32, 16, CH), BF), V((32, 16, CH), BF), V((32, 16, CH), BF), V((32, 16, CH), BF),
             V((2, 16, 16, CH), BF), V((2, 16, 16, CH), BF), V((4, 8, CH), F32),
             V((4, 32, CH), BF), V((4, 32, CH), BF), V((4, 8, CH), F32), V((4, 8, CH), F32),
-            V((512, 512), BF), V((512, 512), BF), V((512, 512), BF), V((256, 256), BF),
+            V((512, 512), BF), V((512, 512), BF), V((512, 512), BF), V((512, 128), BF),
             V((2, 128, 512), BF), V((4, 128, CH), BF), V((4, 128, CH), BF),
-            V((512, CH), BF), V((512, CH), BF), V((128, 896), BF), V((2, 128, 176), BF),
+            V((512, CH), BF), V((128, 896), BF), V((2, 128, 176), BF),
             V((32, CH), F32), V((32, 128), F32), V((2, 128, 128), F32),
             dma((23,)), dma((2,)), dma((2,)), dma((2,)), dma((2,)), dma((2,)), dma((4,)),
             dma((2,)), dma((2,)),

time: 52 us -> 52.1 us (level)
  no operation moved by 1% of the time
where the time goes in v5:
time: 52.1 us; the launch traced here: 52 us
  Pallas kernels  51.3 us (98%)
  between operations  0.65 us (1%)
    pallas_call x1, Pallas kernels, whole(): pl.pallas_call(whole_kernel, out_shape=(V((32, CH), BF), V((32, 2, 128, 1...  49.2 us
    pallas_call x1, Pallas kernels, memory(): pl.pallas_call(memory_kernel, out_shape=tuple((pltpu.HBM(a.shape, a.dtype...  2.11 us

profile of v5, /device:TPU:0, one launch (start us, length us, event | category | flops | bytes accessed | tf_op | source)
XLA Modules:
  0.0 52.0 jit_solution(4674654847855713209)
XLA Ops:
  0.6 49.2 %whole.1 = (bf16[32,512]{1,0:T(8,128)(2,1)S(1)}, f32[32,2,128,128]{3,2,1,0:T(8,128)S(1)}, f32[32,2,128]{2,1,0:T(2,128)S(1)}, f32[2,32]{1,0:T(2,128)S(1)}) custom-call(bf16[32,2048]{1,0:T(8,128)(2,1)} %hidden_h.1, f32[4,2048]{1,0:T(4,128)} %gains_h.1, f32[1,2048]{1,0:T(1,128)} %bitcast.22, s32[2,32]{1,0:T(2,128)} %bitcast.23, f32[2,32]{1,0:T(2,128)} %bitcast.24, ...), custom_call_target="tpu_custom_call" | custom-call | tf_op jit(solution)/shard_map/whole/pallas_call | solution.py:457
  49.9 2.1 %memory.1 = (f32[32,2,128,128]{3,2,1,0:T(8,128)}, f32[32,2,128]{2,1,0:T(2,128)}, f32[2,32]{1,0:T(2,128)}, bf16[32,512]{1,0:T(8,128)(2,1)}) custom-call(f32[32,2,128,128]{3,2,1,0:T(8,128)S(1)} %get-tuple-element.12.matrix, f32[32,2,128]{2,1,0:T(2,128)S(1)} %get-tuple-element.13.norm, f32[2,32]{1,0:T(2,128)S(1)} %get-tuple-element.14.top, ...), custom_call_target="tpu_custom_call" | custom-call | tf_op jit(solution)/shard_map/memory/pallas_call | solution.py:506
